TPU v7x, 1024 devices: a 2x16x16 block of a 4x16x16 slice. The times are simulated.
1024 devices in a mesh: grp: 2 (over x), fs: 16 (over z), tp: 32 (over y, core).
Axes of the slice: x: 2, y: 16, z: 16, core: 2. Of those that a mesh axis runs over, the one named last changes fastest.
The devices are a block of a 4x16x16 slice.
Arguments:
- tokens: bfloat16 [7680, 2048], P(('grp', 'tp')), parts along dimension 0, may hold values from -60 to 60
- route_expert: int32 [7680, 4], P(('grp', 'tp')), parts along dimension 0, may hold values from 0 to 31, all different within a row; in each aligned block of 120 rows (0 to 119, 120 to 239, ...) at most 16 rows name the same one
- route_weight: float32 [7680, 4], P(('grp', 'tp')), parts along dimension 0, may hold values from 0.05 to 1
- norm_gain: float32 [2048], P('tp'), may hold values from 0.1 to 1.9
- gate_train: float32 [32, 2048, 2048], P(None, 'tp', 'fs'), may hold values from -8 to 8
- up_train: float32 [32, 2048, 2048], P(None, 'tp', 'fs'), may hold values from -8 to 8
- down_train: float32 [32, 2048, 2048], P(None, 'tp', 'fs'), may hold values from -0.013671875 to 0.013671875
Outputs:
- gate_serve: bfloat16 [64, 2048, 2048], P(('grp', 'tp'), None, 'fs'), parts along dimension 0
- up_serve: bfloat16 [64, 2048, 2048], P(('grp', 'tp'), None, 'fs'), parts along dimension 0
- down_serve: bfloat16 [64, 2048, 2048], P(('grp', 'tp'), None, 'fs'), parts along dimension 0
- mixed: bfloat16 [7680, 2048], P(('grp', 'tp'), 'fs'), parts along dimension 0
There are 2 independent parts, one for each index of `grp`. A program takes and returns all parts, laid end to end along the dimension named above; an argument that names none is the same for every part. Nothing has to cross between parts.
Inputs may be any that keep to these rules, and one draw needn't show every extreme that they name: `route_expert`: each row names 4 different experts; the rows of one device name each expert at most 16 times.
All inputs are finite; a program needn't handle non-finite values.
Results may differ from a plain program's by a relative error of at most 0.0087.
Values may be sent and summed in bfloat16 or wider, within the bound.
No kernel may reach another device: no remote copies, remote signals or barrier semaphores. Data moves between devices by JAX's collectives and lax.ppermute only.
A program may use at most 32 MiB of HBM per device.

v0:
```python
import jax
import jax.numpy as jnp
from jax import lax
from jax.sharding import PartitionSpec as P

EXPERTS = 32
TOP = 4
CAP = 16


def activate(gate_pre, up_pre):
    clamped = jnp.minimum(gate_pre, 7.0)
    bounded = jnp.clip(up_pre, -7.0, 7.0)
    return (clamped * jax.nn.sigmoid(1.702 * clamped) * (bounded + 1.0)).astype(jnp.bfloat16)


def local(tokens, route_expert, route_weight, norm_gain, gate_train, up_train, down_train):
    gate_local = (gate_train * norm_gain[None, :, None]).astype(jnp.bfloat16)
    up_local = (up_train * norm_gain[None, :, None]).astype(jnp.bfloat16)
    down_local = down_train.astype(jnp.bfloat16)
    gate_serve, up_serve = (
        lax.all_to_all(gate_local, "tp", split_axis=0, concat_axis=1, tiled=True),
        lax.all_to_all(up_local, "tp", split_axis=0, concat_axis=1, tiled=True),
    )
    tp_count = lax.axis_size("tp")
    fs_count = lax.axis_size("fs")
    per_dev = EXPERTS // tp_count
    tok_rows = tokens.shape[0]
    floated = tokens.astype(jnp.float32)
    normed = (
        floated * lax.rsqrt(jnp.mean(floated * floated, axis=-1, keepdims=True) + 1e-06)
    ).astype(jnp.bfloat16)
    flat_expert = route_expert.reshape(-1)
    expert_ids = jnp.arange(EXPERTS, dtype=jnp.int32)
    onehot = (flat_expert[:, None] == expert_ids[None, :]).astype(jnp.int32)
    slot_rank = jnp.sum((jnp.cumsum(onehot, axis=0) - 1) * onehot, axis=1)
    slot_index = flat_expert * CAP + slot_rank
    slot_hit = slot_index[:, None] == jnp.arange(EXPERTS * CAP, dtype=jnp.int32)[None, :]
    placement = slot_hit.reshape(tok_rows, TOP, EXPERTS * CAP).astype(jnp.float32)
    scatter_mat = jnp.sum(placement, axis=1).astype(jnp.bfloat16)
    combine_mat = jnp.sum(placement * route_weight[:, :, None], axis=1)
    col_width = normed.shape[1] // fs_count
    my_block = lax.axis_index("fs")
    column_part = lax.dynamic_slice_in_dim(normed, my_block * col_width, col_width, 1)
    buffer = lax.dot_general(
        scatter_mat, column_part, (((0,), (0,)), ((), ())), preferred_element_type=jnp.float32
    )
    arrived = lax.all_to_all(
        buffer.astype(jnp.bfloat16).reshape(EXPERTS, CAP, column_part.shape[1]),
        "tp",
        split_axis=0,
        concat_axis=0,
        tiled=True,
    )
    arrived = arrived.reshape(tp_count, per_dev, CAP, col_width)
    block_in = lax.all_gather(arrived, "fs", axis=3, tiled=True)
    gate_part = jnp.einsum(
        "secd,edf->secf", block_in, gate_serve, preferred_element_type=jnp.float32
    )
    up_part = jnp.einsum("secd,edf->secf", block_in, up_serve, preferred_element_type=jnp.float32)
    hidden = activate(gate_part, up_part)
    down_serve = lax.all_to_all(down_local, "tp", split_axis=0, concat_axis=1, tiled=True)
    expert_out = jnp.einsum(
        "secf,efd->secd",
        lax.all_gather(hidden, "fs", axis=3, tiled=True),
        down_serve,
        preferred_element_type=jnp.float32,
    ).astype(jnp.bfloat16)
    outgoing = expert_out.reshape(tp_count * per_dev, CAP, down_serve.shape[2])
    returned_rows = lax.all_to_all(outgoing, "tp", split_axis=0, concat_axis=0, tiled=True).reshape(
        EXPERTS * CAP, down_serve.shape[2]
    )
    mixed = jnp.dot(
        combine_mat, returned_rows.astype(jnp.float32), precision=lax.Precision.HIGHEST
    ).astype(jnp.bfloat16)
    return (gate_serve, up_serve, down_serve, mixed)


def solution(mesh):
    return jax.shard_map(
        local,
        mesh=mesh,
        in_specs=(
            P(("grp", "tp"), None),
            P(("grp", "tp"), None),
            P(("grp", "tp"), None),
            P("tp"),
            P(None, "tp", "fs"),
            P(None, "tp", "fs"),
            P(None, "tp", "fs"),
        ),
        out_specs=(
            P(("grp", "tp"), None, "fs"),
            P(("grp", "tp"), None, "fs"),
            P(("grp", "tp"), None, "fs"),
            P(("grp", "tp"), "fs"),
        ),
        check_vma=False,
    )
```

profile of v0, /device:TPU:6, one launch (start us, length us, event | category | flops | bytes accessed | tf_op | source)
XLA Modules:
  0.0 323.6 jit_solution(17860059163243015831)
XLA Ops:
  7.2 0.1 all-gather.6.cloned.1.call-start
  7.3 1.3 convert_element_type.44
  8.6 1.2 multiply_reduce_fusion
  9.8 0.8 copy.54
  10.6 0.1 eq.36
  10.7 1.2 reduce-window.6
  11.9 0.2 slice_reduce_fusion
  12.2 0.1 bitcast_bitcast_fusion
  12.3 0.1 reduce_sum.39
  12.4 0.1 copy.57
  12.5 0.2 convert_reduce_fusion
  12.8 0.3 convolution_convert_fusion
  13.0 31.5 %all_to_all.46 = bf16[32,16,128]{2,1,0:T(8,128)(2,1)S(1)} all-to-all(bf16[32,16,128]{2,1,0:T(8,128)(2,1)S(1)} %bitcast.58), channel_id=1, replica_groups=mesh['grp'=2,'fs'=16,'tp'=32] {'tp'}, dimensions={0} | all-to-all | bytes 262144 | tf_op jit(solution)/shard_map/all_to_all | solution.py:48
  44.5 0.7 copy.58
  45.3 1.1 multiply_convert_fusion
  46.3 37.1 %all_to_all.47 = bf16[32,64,128]{2,1,0:T(8,128)(2,1)S(1)} all-to-all(bf16[32,64,128]{2,1,0:T(8,128)(2,1)S(1)} %get-tuple-element.7), channel_id=1, replica_groups=mesh['grp'=2,'fs'=16,'tp'=32] {'tp'}, dimensions={0} | all-to-all | bytes 1048576 | tf_op jit(solution)/shard_map/all_to_all | solution.py:22
  83.4 4.8 %all-to-all-start.1 = ((bf16[32,64,128]{2,1,0:T(8,128)(2,1)}), bf16[32,64,128]{2,1,0:T(8,128)(2,1)S(1)}, u32[]{:S(2)}, u32[]{:S(2)}) async-start(bf16[32,64,128]{2,1,0:T(8,128)(2,1)} %get-tuple-element.6), calls=%async_computation.1 | async-start | bytes 1048576 | tf_op jit(solution)/shard_map/all_to_all | solution.py:23
  88.2 0.1 all-gather.4.cloned.1.call-start
  88.3 106.0 %all-gather.6.cloned.1.call-done = bf16[32,16,2048]{2,0,1:T(8,128)(2,1)} async-done(((bf16[32,16,128]{2,0,1:T(8,128)(2,1)}), bf16[32,16,2048]{2,0,1:T(8,128)(2,1)}) %all-gather.6.cloned.1.call-update) | async-done | bytes 2097168 | tf_op jit(solution)/shard_map/all_gather | solution.py:56
  194.3 2.3 fusion.2
  196.6 3.1 fusion.9
  199.8 0.1 convert_element_type.41
  199.9 44.8 %all_to_all.48 = bf16[32,64,128]{2,1,0:T(8,128)(2,1)S(1)} all-to-all(bf16[32,64,128]{2,1,0:T(8,128)(2,1)S(1)} %convert_element_type.41), channel_id=1, replica_groups=mesh['grp'=2,'fs'=16,'tp'=32] {'tp'}, dimensions={0} | all-to-all | bytes 1048576 | tf_op jit(solution)/shard_map/all_to_all | solution.py:62
  244.6 35.7 %all-gather.4.cloned.1.call-done = bf16[32,1,16,2048]{3,0,2,1:T(8,128)(2,1)} async-done(((bf16[32,1,16,128]{3,0,2,1:T(8,128)(2,1)}), bf16[32,1,16,2048]{3,0,2,1:T(8,128)(2,1)}) %all-gather.4.cloned.1.call-update) | async-done | bytes 2097168 | tf_op jit(solution)/shard_map/all_gather | solution.py:65
  280.3 2.3 fusion.6
  282.7 0.7 copy.59
  283.4 13.6 %all-to-all-start.4 = ((bf16[32,16,128]{2,1,0:T(8,128)(2,1)}), bf16[32,16,128]{2,1,0:T(8,128)(2,1)S(1)}, u32[]{:S(2)}, u32[]{:S(2)}) async-start(bf16[32,16,128]{2,1,0:T(8,128)(2,1)} %copy.59), calls=%async_computation.4 | async-start | bytes 262144 | tf_op jit(solution)/shard_map/all_to_all | solution.py:70
  297.0 16.5 %all-to-all-done.4 = bf16[32,16,128]{2,1,0:T(8,128)(2,1)S(1)} async-done(((bf16[32,16,128]{2,1,0:T(8,128)(2,1)}), bf16[32,16,128]{2,1,0:T(8,128)(2,1)S(1)}, u32[]{:S(2)}, u32[]{:S(2)}) %all-to-all-start.4) | async-done | bytes 131104 | tf_op jit(solution)/shard_map/all_to_all | solution.py:70
  313.5 0.9 convolution_convert_fusion.1
  314.4 0.8 copy.67
  315.1 0.8 copy.68
  315.9 0.8 copy.69
  (22 shorter events, 0.3 us)
Async XLA Ops:
  7.2 5.3 %copy-start.3 = (s32[120,4]{0,1:T(4,128)S(1)}, s32[120,4]{0,1:T(4,128)}, u32[]{:S(2)}) copy-start(s32[120,4]{0,1:T(4,128)} %param.8) | copy-start | bytes 5764
  7.2 5.3 %copy-start.4 = (f32[120,4]{0,1:T(4,128)S(1)}, f32[120,4]{0,1:T(4,128)}, u32[]{:S(2)}) copy-start(f32[120,4]{0,1:T(4,128)} %param.9) | copy-start | bytes 5764
  7.2 38.0 %copy-start.5 = (f32[64]{0:T(128)S(1)}, f32[64]{0:T(128)}, u32[]{:S(2)}) copy-start(f32[64]{0:T(128)} %param.10) | copy-start | bytes 772
  7.2 38.0 %copy-start.2 = (f32[32,64,128]{2,1,0:T(8,128)S(1)}, f32[32,64,128]{2,1,0:T(8,128)}, u32[]{:S(2)}) copy-start(f32[32,64,128]{2,1,0:T(8,128)} %param.11) | copy-start | bytes 3145732
  7.2 38.0 %copy-start.1 = (f32[32,64,128]{2,1,0:T(8,128)S(1)}, f32[32,64,128]{2,1,0:T(8,128)}, u32[]{:S(2)}) copy-start(f32[32,64,128]{2,1,0:T(8,128)} %param.12) | copy-start | bytes 3145732
  7.2 187.1 %all-gather.6.cloned.1.call-start = ((), (), s32[]{:S(2)}) async-start(), calls=%async_computation.6 | async-start | bytes 2228224 | tf_op jit(solution)/shard_map/all_gather | solution.py:56
  83.4 113.2 %all-to-all-start.1 = ((bf16[32,64,128]{2,1,0:T(8,128)(2,1)}), bf16[32,64,128]{2,1,0:T(8,128)(2,1)S(1)}, u32[]{:S(2)}, u32[]{:S(2)}) async-start(bf16[32,64,128]{2,1,0:T(8,128)(2,1)} %get-tuple-element.6), calls=%async_computation.1 | async-start | bytes 1048576 | tf_op jit(solution)/shard_map/all_to_all | solution.py:23
  88.2 192.1 %all-gather.4.cloned.1.call-start = ((), (), s32[]{:S(2)}) async-start(), calls=%async_computation.5 | async-start | bytes 2228224 | tf_op jit(solution)/shard_map/all_gather | solution.py:65
  196.6 3.1 copy-start
  283.4 30.1 %all-to-all-start.4 = ((bf16[32,16,128]{2,1,0:T(8,128)(2,1)}), bf16[32,16,128]{2,1,0:T(8,128)(2,1)S(1)}, u32[]{:S(2)}, u32[]{:S(2)}) async-start(bf16[32,16,128]{2,1,0:T(8,128)(2,1)} %copy.59), calls=%async_computation.4 | async-start | bytes 262144 | tf_op jit(solution)/shard_map/all_to_all | solution.py:70
Sparse Core Ops, SparseCore 0:
  45.4 148.9 all-gather.5
  199.9 80.4 all-gather.3
where the time goes:
time: 324 us
  waiting for transfers between devices  158 us (49%)
  blocking collectives  113 us (35%)
  starting transfers between devices  18.6 us (6%)
  between operations  14.3 us (4%)
  matrix products  8.77 us (3%)
  other arithmetic  5.23 us (2%)
  local copies, waits for them, and re-layouts  5.1 us (2%)
    all_gather x1, waiting for transfers between devices, local(): block_in = lax.all_gather(arrived, 'fs', axis=3, tiled=True)  106 us
    all_to_all x1, blocking collectives, local(): lax.all_to_all(down_local, 'tp', split_axis=0, concat_axis=1, tiled=True)  44.8 us
    all_to_all x1, blocking collectives, local(): lax.all_to_all(gate_local, 'tp', split_axis=0, concat_axis=1, tiled=True)  37.1 us
    all_gather x1, waiting for transfers between devices, local(): lax.all_gather(hidden, 'fs', axis=3, tiled=True)  35.7 us
    all_to_all x1, blocking collectives, local(): lax.all_to_all(buffer.astype(jnp.bfloat16).reshape(EXPERTS, CAP, column_p...  31.5 us
    all_to_all x1, waiting for transfers between devices, local(): lax.all_to_all(outgoing, 'tp', split_axis=0, concat_axis=0, tiled=True)  16.5 us
    all_to_all x1, starting transfers between devices, local(): lax.all_to_all(outgoing, 'tp', split_axis=0, concat_axis=0, tiled=True)  13.6 us
  transfers between devices with their start and end apart: 4, of which 3 were waited for; matrix products, arithmetic and copies ran while one was open for 1% of the time, Pallas kernels for 0%

commit v1 on v0

v1 whole, which is shorter than its diff:
```python
import functools

import jax
import jax.numpy as jnp
from jax import lax
from jax.experimental import pallas as pl
from jax.experimental.pallas import tpu as pltpu
from jax.sharding import PartitionSpec as P


EXPERTS = 32
TOP = 4
CAP = 16
SUB = 4
F32 = jnp.float32
BF16 = jnp.bfloat16


def vm():
    return pl.BlockSpec(memory_space=pltpu.VMEM)


def sm():
    return pl.BlockSpec(memory_space=pltpu.SMEM)


def prep_kernel(block, tokens, route_t, weight_t, buffer, comb_hi, comb_lo):
    rows, _ = tokens.shape
    floated = tokens[...].astype(F32)
    inv = lax.rsqrt(jnp.mean(floated * floated, axis=-1, keepdims=True) + 1e-06)
    cols = buffer.shape[1]
    part = tokens[:, pl.ds(pl.multiple_of(block[0] * cols, cols), cols)].astype(F32)
    normed = (part * inv).astype(BF16)
    expert = lax.broadcasted_iota(jnp.int32, (EXPERTS, rows), 0)
    named = jnp.zeros((EXPERTS, rows), F32)
    weight = jnp.zeros((EXPERTS, rows), F32)
    for k in range(TOP):
        hit = route_t[k : k + 1, :] == expert
        named = named + jnp.where(hit, 1.0, 0.0)
        weight = weight + jnp.where(hit, weight_t[k : k + 1, :], 0.0)
    earlier = lax.broadcasted_iota(jnp.int32, (rows, rows), 0) < lax.broadcasted_iota(
        jnp.int32, (rows, rows), 1
    )
    rank = jnp.dot(
        named.astype(BF16),
        jnp.where(earlier, 1.0, 0.0).astype(BF16),
        preferred_element_type=F32,
    )
    rank = jnp.where(named > 0.5, rank, -1.0)
    slot = lax.broadcasted_iota(jnp.int32, (EXPERTS, CAP, rows), 1).astype(F32)
    taken = rank[:, None, :] == slot
    scatter = jnp.where(taken, 1.0, 0.0).reshape(EXPERTS * CAP, rows)
    buffer[...] = jnp.dot(scatter.astype(BF16), normed, preferred_element_type=F32).astype(BF16)
    comb = jnp.where(taken, weight[:, None, :], 0.0).reshape(EXPERTS * CAP, rows)
    high = comb.astype(BF16)
    comb_hi[...] = high
    comb_lo[...] = (comb - high.astype(F32)).astype(BF16)


def pieces(own, below, above, below2, above2, res, stride):
    half = SUB // 2
    out = []
    for ref, r in ((own, res), (below, (res + stride - 1) % stride), (above, (res + 1) % stride)):
        for k in range(0, SUB, 2):
            out.append((ref, k, k, r))
    for k in range(0, half, 2):
        out.append((below2, k, k, (res + 2) % stride))
        out.append((above2, k, half + k, (res + 2) % stride))
    return out


def passed_on(pairs, sems):
    return [pltpu.make_async_copy(src, dst, sems.at[i]) for i, (src, dst) in enumerate(pairs)]


def block_of(w, k, r, stride, at, size):
    per = w.shape[0] // (SUB * stride)
    first = (k * stride + r) * per
    return jnp.concatenate([w[first + j, at : at + size, :] for j in range(per)], axis=0)


def gate_up_kernel(
    res, own, below, above, below2, above2, weight, hidden, gate_out, up_out, rhs, sems, *, stride
):
    rows, width = hidden.shape
    size = weight.shape[1] // 2
    copies = passed_on(
        ((weight.at[:, :size, :], gate_out), (weight.at[:, size:, :], up_out)), sems
    )
    for c in copies:
        c.start()
    order = pieces(own, below, above, below2, above2, res[0], stride)
    for n, (_, _, wk, r) in enumerate(order):
        for j in range(2):
            half = rhs.at[n, j * (rhs.shape[1] // 2) : (j + 1) * (rhs.shape[1] // 2), :]
            half[:, :width] = block_of(weight, wk + j, r, stride, 0, size)
            half[:, width:] = block_of(weight, wk + j, r, stride, size, size)
    step = 128

    def one(i, carry):
        at = pl.ds(pl.multiple_of(i * step, step), step)
        acc = jnp.zeros((step, 2 * width), F32)
        for n, (ref, k, _, _) in enumerate(order):
            lhs = jnp.concatenate([ref[k, at, :], ref[k + 1, at, :]], axis=1)
            acc = acc + jnp.dot(lhs, rhs[n], preferred_element_type=F32)
        g = jnp.minimum(acc[:, :width], 7.0)
        u = jnp.clip(acc[:, width:], -7.0, 7.0)
        hidden[at, :] = (g * jax.nn.sigmoid(1.702 * g) * (u + 1.0)).astype(BF16)
        return carry

    lax.fori_loop(0, rows // step, one, 0)
    for c in copies:
        c.wait()


def down_kernel(
    res, own, below, above, below2, above2, weight, out, down_out, rhs, sems, *, stride
):
    rows, width = out.shape
    copies = passed_on(((weight, down_out),), sems)
    for c in copies:
        c.start()
    order = pieces(own, below, above, below2, above2, res[0], stride)
    for n, (_, _, wk, r) in enumerate(order):
        for j in range(2):
            half = rhs.at[n, j * (rhs.shape[1] // 2) : (j + 1) * (rhs.shape[1] // 2), :]
            half[...] = block_of(weight, wk + j, r, stride, 0, weight.shape[1])
    step = 128

    def one(i, carry):
        at = pl.ds(pl.multiple_of(i * step, step), step)
        acc = jnp.zeros((step, width), F32)
        for n, (ref, k, _, _) in enumerate(order):
            lhs = jnp.concatenate([ref[k, at, :], ref[k + 1, at, :]], axis=1)
            acc = acc + jnp.dot(lhs, rhs[n], preferred_element_type=F32)
        out[at, :] = acc.astype(BF16)
        return carry

    lax.fori_loop(0, rows // step, one, 0)
    for c in copies:
        c.wait()


def combine_kernel(comb_hi, comb_lo, rows, mixed):
    dims = (((0,), (0,)), ((), ()))
    acc = lax.dot_general(comb_hi[...], rows[...], dims, preferred_element_type=F32)
    acc = acc + lax.dot_general(comb_lo[...], rows[...], dims, preferred_element_type=F32)
    mixed[...] = acc.astype(BF16)


def exchange(x):
    return lax.all_to_all(x, "tp", split_axis=0, concat_axis=0, tiled=True)


def after(x, *others):
    return lax.optimization_barrier((x, *others))[0]


def gather(block):
    count = lax.axis_size("fs")
    stride = count // SUB
    groups = [[i + stride * j for j in range(SUB)] for i in range(stride)]
    own = lax.all_gather(block, "fs", axis=0, axis_index_groups=groups)

    def shift(x, by):
        return lax.ppermute(x, "fs", [(i, (i + by) % count) for i in range(count)])

    half = SUB // 2
    return (
        own,
        shift(own, 1),
        shift(own, -1),
        shift(own[:half], 2),
        shift(own[half:], -2),
    )


def body(tokens, route_expert, route_weight, norm_gain, gate_train, up_train, down_train):
    tp_count = lax.axis_size("tp")
    fs_count = lax.axis_size("fs")
    stride = fs_count // SUB
    tok_rows, width = tokens.shape
    cols = width // fs_count
    slots = EXPERTS * CAP
    my_block = lax.axis_index("fs").astype(jnp.int32)
    res = (my_block % stride).reshape(1)

    buffer, comb_hi, comb_lo = pl.pallas_call(
        prep_kernel,
        in_specs=[sm(), vm(), vm(), vm()],
        out_specs=[vm(), vm(), vm()],
        out_shape=[
            jax.ShapeDtypeStruct((slots, cols), BF16),
            jax.ShapeDtypeStruct((slots, tok_rows), BF16),
            jax.ShapeDtypeStruct((slots, tok_rows), BF16),
        ],
        name="prep",
    )(my_block.reshape(1), tokens, route_expert.T, route_weight.T)
    arrived = exchange(buffer.reshape(EXPERTS, CAP, cols)).reshape(slots, cols)

    gain = norm_gain[None, :, None]
    packed = jnp.concatenate(
        [(gate_train * gain).astype(BF16), (up_train * gain).astype(BF16)], axis=1
    )
    both = exchange(after(packed, arrived))
    served = jax.ShapeDtypeStruct(down_train.shape, BF16)
    hbm = pl.BlockSpec(memory_space=pl.ANY)
    pairs = fs_count // 2

    hidden, gate_serve, up_serve = pl.pallas_call(
        functools.partial(gate_up_kernel, stride=stride),
        in_specs=[sm()] + [vm()] * 6,
        out_specs=[vm(), hbm, hbm],
        out_shape=[jax.ShapeDtypeStruct((slots, both.shape[2]), BF16), served, served],
        scratch_shapes=[
            pltpu.VMEM((pairs, 2 * cols, 2 * both.shape[2]), BF16),
            pltpu.SemaphoreType.DMA((2,)),
        ],
        name="gate_up",
    )(res, *gather(arrived), both)
    arrived_down = exchange(after(down_train.astype(BF16), both))
    expert_out, down_serve = pl.pallas_call(
        functools.partial(down_kernel, stride=stride),
        in_specs=[sm()] + [vm()] * 6,
        out_specs=[vm(), hbm],
        out_shape=[jax.ShapeDtypeStruct((slots, down_train.shape[2]), BF16), served],
        scratch_shapes=[
            pltpu.VMEM((pairs, 2 * both.shape[2], down_train.shape[2]), BF16),
            pltpu.SemaphoreType.DMA((1,)),
        ],
        name="down",
    )(res, *gather(hidden), arrived_down)
    returned = exchange(expert_out.reshape(tp_count, slots // tp_count, -1)).reshape(slots, -1)
    mixed = pl.pallas_call(
        combine_kernel,
        in_specs=[vm()] * 3,
        out_specs=vm(),
        out_shape=jax.ShapeDtypeStruct((tok_rows, returned.shape[1]), BF16),
        name="combine",
    )(comb_hi, comb_lo, returned)

    def whole(w):
        return w.reshape(1, -1, w.shape[-1])

    return (whole(gate_serve), whole(up_serve), whole(down_serve), mixed)


def solution(mesh):
    return jax.shard_map(
        body,
        mesh=mesh,
        in_specs=(
            P(("grp", "tp"), None),
            P(("grp", "tp"), None),
            P(("grp", "tp"), None),
            P("tp"),
            P(None, "tp", "fs"),
            P(None, "tp", "fs"),
            P(None, "tp", "fs"),
        ),
        out_specs=(
            P(("grp", "tp"), None, "fs"),
            P(("grp", "tp"), None, "fs"),
            P(("grp", "tp"), None, "fs"),
            P(("grp", "tp"), "fs"),
        ),
        check_vma=False,
    )
```

time: 324 us -> 329 us (1.015)
  the two profiles are of different devices: /device:TPU:6 before, /device:TPU:5 now
where the time goes in v1:
time: 329 us; the launch traced here: 328 us
  starting transfers between devices  135 us (41%)
  waiting for transfers between devices  98.4 us (30%)
  blocking collectives  75.6 us (23%)
  Pallas kernels  11.6 us (4%)
  other arithmetic  3.8 us (1%)
    all_to_all x3, starting transfers between devices, exchange(): return lax.all_to_all(x, 'tp', split_axis=0, concat_axis=0, tiled=True)  97.5 us
    all_to_all x3, waiting for transfers between devices, exchange(): return lax.all_to_all(x, 'tp', split_axis=0, concat_axis=0, tiled=True)  68.5 us
    all_gather x2, blocking collectives, gather(): own = lax.all_gather(block, 'fs', axis=0, axis_index_groups=groups)  43.9 us
    ppermute x8, starting transfers between devices, shift(): return lax.ppermute(x, 'fs', [(i, (i + by) % count) for i in range(count)])  37.1 us
    all_to_all x1, blocking collectives, exchange(): return lax.all_to_all(x, 'tp', split_axis=0, concat_axis=0, tiled=True)  31.7 us
    ppermute x8, waiting for transfers between devices, shift(): return lax.ppermute(x, 'fs', [(i, (i + by) % count) for i in range(count)])  29.9 us
  transfers between devices with their start and end apart: 11, of which 6 were waited for; matrix products, arithmetic and copies ran while one was open for 0% of the time, Pallas kernels for 2%

profile of v1, /device:TPU:5, one launch (start us, length us, event | category | flops | bytes accessed | tf_op | source)
XLA Modules:
  0.0 328.0 jit_solution(11386320764115122280)
XLA Ops:
  0.6 1.8 multiply_convert_fusion.1
  2.5 1.1 pad_maximum_fusion
  3.5 87.4 %all-to-all-start.1 = ((bf16[32,128,128]{2,1,0:T(8,128)(2,1)}), bf16[32,128,128]{2,1,0:T(8,128)(2,1)S(1)}, u32[]{:S(2)}, u32[]{:S(2)}) async-start(bf16[32,128,128]{2,1,0:T(8,128)(2,1)} %pad_maximum_fusion), calls=%async_computation.1 | async-start | bytes 2097152 | tf_op jit(solution)/shard_map/all_to_all | solution.py:152
  91.0 2.1 prep.1
  93.1 53.5 %all-to-all-done.1.weight = bf16[32,128,128]{2,1,0:T(8,128)(2,1)S(1)} async-done(((bf16[32,128,128]{2,1,0:T(8,128)(2,1)}), bf16[32,128,128]{2,1,0:T(8,128)(2,1)S(1)}, u32[]{:S(2)}, u32[]{:S(2)}) %all-to-all-start.1) | async-done | bytes 1048608 | tf_op jit(solution)/shard_map/all_to_all | solution.py:152
  146.6 4.9 %all-to-all-start = ((bf16[32,16,128]{2,1,0:T(8,128)(2,1)}), bf16[32,16,128]{2,1,0:T(8,128)(2,1)S(1)}, u32[]{:S(2)}, u32[]{:S(2)}) async-start(bf16[32,16,128]{2,1,0:T(8,128)(2,1)} %bitcast.21), calls=%async_computation | async-start | bytes 262144 | tf_op jit(solution)/shard_map/all_to_all | solution.py:152
  151.5 0.9 convert_element_type.11
  152.4 15.0 %all-to-all-done = bf16[32,16,128]{2,1,0:T(8,128)(2,1)S(1)} async-done(((bf16[32,16,128]{2,1,0:T(8,128)(2,1)}), bf16[32,16,128]{2,1,0:T(8,128)(2,1)S(1)}, u32[]{:S(2)}, u32[]{:S(2)}) %all-to-all-start) | async-done | bytes 131104 | tf_op jit(solution)/shard_map/all_to_all | solution.py:152
  167.4 5.3 %all-to-all-start.2 = ((bf16[32,64,128]{2,1,0:T(8,128)(2,1)}), bf16[32,64,128]{2,1,0:T(8,128)(2,1)S(1)}, u32[]{:S(2)}, u32[]{:S(2)}) async-start(bf16[32,64,128]{2,1,0:T(8,128)(2,1)} %convert_element_type.11), calls=%async_computation.2 | async-start | bytes 1048576 | tf_op jit(solution)/shard_map/all_to_all | solution.py:152
  172.6 19.3 %all_gather.9.own = bf16[4,512,128]{2,1,0:T(8,128)(2,1)S(1)} all-gather(bf16[1,512,128]{2,1,0:T(8,128)(2,1)S(1)} %bitcast.17), channel_id=1, replica_groups={{0,128,256,384},{32,160,288,416},{64,192,320,448},{96,224,352,480},{1,1..., dimensions={0}, use_global_device_ids=true | all-gather | bytes 655360 | tf_op jit(solution)/shard_map/all_gather | solution.py:163
  192.0 1.9 collective-permute-start
  193.9 13.7 %collective-permute-start.1 = (bf16[4,512,128]{2,1,0:T(8,128)(2,1)S(1)}, bf16[4,512,128]{2,1,0:T(8,128)(2,1)S(1)}, u32[]{:S(2)}, u32[]{:S(2)}) collective-permute-start(bf16[4,512,128]{2,1,0:T(8,128)(2,1)S(1)} %all_gather.9.own), channel_id=1, source_target_pairs={{0,480},{32,0},{64,32},{96,64},{128,96},{160,128},{192,160},{224,1... | collective-permute-start | bytes 1572872 | tf_op jit(solution)/shard_map/ppermute | solution.py:166
  207.7 2.0 collective-permute-start.2
  209.7 5.5 %collective-permute-start.3 = (bf16[2,512,128]{2,1,0:T(8,128)(2,1)S(1)}, bf16[2,512,128]{2,1,0:T(8,128)(2,1)S(1)}, u32[]{:S(2)}, u32[]{:S(2)}) collective-permute-start(bf16[2,512,128]{2,1,0:T(8,128)(2,1)S(1)} %get-tuple-element.24), channel_id=1, source_target_pairs={{0,448},{32,480},{64,0},{96,32},{128,64},{160,96},{192,128},{224,1... | collective-permute-start | bytes 786440 | tf_op jit(solution)/shard_map/ppermute | solution.py:166
  215.2 9.9 %collective-permute-done.2.below2 = bf16[2,512,128]{2,1,0:T(8,128)(2,1)S(1)} collective-permute-done((bf16[2,512,128]{2,1,0:T(8,128)(2,1)S(1)}, bf16[2,512,128]{2,1,0:T(8,128)(2,1)S(1)}, u32[]{:S(2)}, u32[]{:S(2)}) %collective-permute-start.2) | collective-permute-done | bytes 262176 | tf_op jit(solution)/shard_map/ppermute | solution.py:166
  225.1 3.4 %collective-permute-done.3.above2 = bf16[2,512,128]{2,1,0:T(8,128)(2,1)S(1)} collective-permute-done((bf16[2,512,128]{2,1,0:T(8,128)(2,1)S(1)}, bf16[2,512,128]{2,1,0:T(8,128)(2,1)S(1)}, u32[]{:S(2)}, u32[]{:S(2)}) %collective-permute-start.3) | collective-permute-done | bytes 262176 | tf_op jit(solution)/shard_map/ppermute | solution.py:166
  228.6 0.7 copy-done.10
  229.2 0.2 copy-done.5
  229.6 4.0 %gate_up.1 = (bf16[512,128]{1,0:T(8,128)(2,1)}, bf16[32,64,128]{2,1,0:T(8,128)(2,1)}, bf16[32,64,128]{2,1,0:T(8,128)(2,1)}) custom-call(s32[1]{0:T(128)} %bitcast.res, bf16[4,512,128]{2,1,0:T(8,128)(2,1)} %copy-done, bf16[4,512,128]{2,1,0:T(8,128)(2,1)} %copy-done.5, bf16[4,512,128]{2,1,0:T(8,128)(2,1)} %copy-done.6, bf16[2,512,128]{2,1,0:T(8,128)(2,1)} %copy-done.9, ...), custom_call_target="tpu_custom_call" | custom-call | tf_op jit(solution)/shard_map/gate_up/pallas_call | solution.py:210
  233.6 24.6 %all-gather = bf16[2048,128]{1,0:T(8,128)(2,1)S(1)} all-gather(bf16[512,128]{1,0:T(8,128)(2,1)} %get-tuple-element.16), channel_id=2, replica_groups={{0,128,256,384},{32,160,288,416},{64,192,320,448},{96,224,352,480},{1,1..., dimensions={0}, use_global_device_ids=true | all-gather | bytes 655360 | tf_op jit(solution)/shard_map/all_gather | solution.py:163
  258.2 1.9 collective-permute-start.4
  260.2 4.6 %collective-permute-start.5 = (bf16[4,512,128]{2,1,0:T(8,128)(2,1)S(1)}, bf16[4,512,128]{2,1,0:T(8,128)(2,1)S(1)}, u32[]{:S(2)}, u32[]{:S(2)}) collective-permute-start(bf16[4,512,128]{2,1,0:T(8,128)(2,1)S(1)} %bitcast.15), channel_id=1, source_target_pairs={{0,480},{32,0},{64,32},{96,64},{128,96},{160,128},{192,160},{224,1... | collective-permute-start | bytes 1572872 | tf_op jit(solution)/shard_map/ppermute | solution.py:166
  264.8 4.1 %collective-permute-start.6 = (bf16[2,512,128]{2,1,0:T(8,128)(2,1)S(1)}, bf16[2,512,128]{2,1,0:T(8,128)(2,1)S(1)}, u32[]{:S(2)}, u32[]{:S(2)}) collective-permute-start(bf16[2,512,128]{2,1,0:T(8,128)(2,1)S(1)} %bitcast.20), channel_id=1, source_target_pairs={{0,64},{32,96},{64,128},{96,160},{128,192},{160,224},{192,256},{22... | collective-permute-start | bytes 786440 | tf_op jit(solution)/shard_map/ppermute | solution.py:166
  268.9 3.4 %collective-permute-start.7 = (bf16[2,512,128]{2,1,0:T(8,128)(2,1)S(1)}, bf16[2,512,128]{2,1,0:T(8,128)(2,1)S(1)}, u32[]{:S(2)}, u32[]{:S(2)}) collective-permute-start(bf16[2,512,128]{2,1,0:T(8,128)(2,1)S(1)} %bitcast.19), channel_id=1, source_target_pairs={{0,448},{32,480},{64,0},{96,32},{128,64},{160,96},{192,128},{224,1... | collective-permute-start | bytes 786440 | tf_op jit(solution)/shard_map/ppermute | solution.py:166
  272.3 7.0 %collective-permute-done.6.below2 = bf16[2,512,128]{2,1,0:T(8,128)(2,1)S(1)} collective-permute-done((bf16[2,512,128]{2,1,0:T(8,128)(2,1)S(1)}, bf16[2,512,128]{2,1,0:T(8,128)(2,1)S(1)}, u32[]{:S(2)}, u32[]{:S(2)}) %collective-permute-start.6) | collective-permute-done | bytes 262176 | tf_op jit(solution)/shard_map/ppermute | solution.py:166
  279.3 9.6 %collective-permute-done.7.above2 = bf16[2,512,128]{2,1,0:T(8,128)(2,1)S(1)} collective-permute-done((bf16[2,512,128]{2,1,0:T(8,128)(2,1)S(1)}, bf16[2,512,128]{2,1,0:T(8,128)(2,1)S(1)}, u32[]{:S(2)}, u32[]{:S(2)}) %collective-permute-start.7) | collective-permute-done | bytes 262176 | tf_op jit(solution)/shard_map/ppermute | solution.py:166
  288.9 0.7 copy-done.12
  289.7 0.2 copy-done.8
  289.9 0.8 copy-done.3
  290.8 3.6 %down.1 = (bf16[512,128]{1,0:T(8,128)(2,1)}, bf16[32,64,128]{2,1,0:T(8,128)(2,1)}) custom-call(s32[1]{0:T(128)} %bitcast.res, bf16[4,512,128]{2,1,0:T(8,128)(2,1)} %bitcast.16, bf16[4,512,128]{2,1,0:T(8,128)(2,1)} %copy-done.7, bf16[4,512,128]{2,1,0:T(8,128)(2,1)} %copy-done.8, bf16[2,512,128]{2,1,0:T(8,128)(2,1)} %copy-done.11, ...), custom_call_target="tpu_custom_call" | custom-call | tf_op jit(solution)/shard_map/down/pallas_call | solution.py:222
  294.3 31.7 %all_to_all.20 = bf16[32,16,128]{2,1,0:T(8,128)(2,1)} all-to-all(bf16[32,16,128]{2,1,0:T(8,128)(2,1)} %bitcast.22), channel_id=1, replica_groups=mesh['grp'=2,'fs'=16,'tp'=32] {'tp'}, dimensions={0} | all-to-all | bytes 262144 | tf_op jit(solution)/shard_map/all_to_all | solution.py:152
  326.1 1.9 combine.1
  (28 shorter events, 0.5 us)
Async XLA Ops:
  3.5 147.9 %copy-start.4 = (f32[32,64,128]{2,1,0:T(8,128)S(1)}, f32[32,64,128]{2,1,0:T(8,128)}, u32[]{:S(2)}) copy-start(f32[32,64,128]{2,1,0:T(8,128)} %param.13) | copy-start | bytes 3145732
  3.5 143.0 %all-to-all-start.1 = ((bf16[32,128,128]{2,1,0:T(8,128)(2,1)}), bf16[32,128,128]{2,1,0:T(8,128)(2,1)S(1)}, u32[]{:S(2)}, u32[]{:S(2)}) async-start(bf16[32,128,128]{2,1,0:T(8,128)(2,1)} %pad_maximum_fusion), calls=%async_computation.1 | async-start | bytes 2097152 | tf_op jit(solution)/shard_map/all_to_all | solution.py:152
  146.6 20.8 %copy-start.2 = (bf16[32,128,128]{2,1,0:T(8,128)(2,1)}, bf16[32,128,128]{2,1,0:T(8,128)(2,1)S(1)}, u32[]{:S(2)}) copy-start(bf16[32,128,128]{2,1,0:T(8,128)(2,1)S(1)} %all-to-all-done.1.weight) | copy-start | bytes 3145732
  146.6 20.8 %all-to-all-start = ((bf16[32,16,128]{2,1,0:T(8,128)(2,1)}), bf16[32,16,128]{2,1,0:T(8,128)(2,1)S(1)}, u32[]{:S(2)}, u32[]{:S(2)}) async-start(bf16[32,16,128]{2,1,0:T(8,128)(2,1)} %bitcast.21), calls=%async_computation | async-start | bytes 262144 | tf_op jit(solution)/shard_map/all_to_all | solution.py:152
  167.4 121.5 %all-to-all-start.2 = ((bf16[32,64,128]{2,1,0:T(8,128)(2,1)}), bf16[32,64,128]{2,1,0:T(8,128)(2,1)S(1)}, u32[]{:S(2)}, u32[]{:S(2)}) async-start(bf16[32,64,128]{2,1,0:T(8,128)(2,1)} %convert_element_type.11), calls=%async_computation.2 | async-start | bytes 1048576 | tf_op jit(solution)/shard_map/all_to_all | solution.py:152
  192.0 36.6 %copy-start = (bf16[4,512,128]{2,1,0:T(8,128)(2,1)}, bf16[4,512,128]{2,1,0:T(8,128)(2,1)S(1)}, u32[]{:S(2)}) copy-start(bf16[4,512,128]{2,1,0:T(8,128)(2,1)S(1)} %all_gather.9.own) | copy-start | bytes 1572868
  192.0 36.6 %collective-permute-start = (bf16[4,512,128]{2,1,0:T(8,128)(2,1)S(1)}, bf16[4,512,128]{2,1,0:T(8,128)(2,1)S(1)}, u32[]{:S(2)}, u32[]{:S(2)}) collective-permute-start(bf16[4,512,128]{2,1,0:T(8,128)(2,1)S(1)} %all_gather.9.own), channel_id=1, source_target_pairs={{0,32},{32,64},{64,96},{96,128},{128,160},{160,192},{192,224},{224... | collective-permute-start | bytes 1572872 | tf_op jit(solution)/shard_map/ppermute | solution.py:166
  193.9 34.6 %collective-permute-start.1 = (bf16[4,512,128]{2,1,0:T(8,128)(2,1)S(1)}, bf16[4,512,128]{2,1,0:T(8,128)(2,1)S(1)}, u32[]{:S(2)}, u32[]{:S(2)}) collective-permute-start(bf16[4,512,128]{2,1,0:T(8,128)(2,1)S(1)} %all_gather.9.own), channel_id=1, source_target_pairs={{0,480},{32,0},{64,32},{96,64},{128,96},{160,128},{192,160},{224,1... | collective-permute-start | bytes 1572872 | tf_op jit(solution)/shard_map/ppermute | solution.py:166
  207.7 17.4 %collective-permute-start.2 = (bf16[2,512,128]{2,1,0:T(8,128)(2,1)S(1)}, bf16[2,512,128]{2,1,0:T(8,128)(2,1)S(1)}, u32[]{:S(2)}, u32[]{:S(2)}) collective-permute-start(bf16[2,512,128]{2,1,0:T(8,128)(2,1)S(1)} %get-tuple-element.25), channel_id=1, source_target_pairs={{0,64},{32,96},{64,128},{96,160},{128,192},{160,224},{192,256},{22... | collective-permute-start | bytes 786440 | tf_op jit(solution)/shard_map/ppermute | solution.py:166
  209.7 18.9 %collective-permute-start.3 = (bf16[2,512,128]{2,1,0:T(8,128)(2,1)S(1)}, bf16[2,512,128]{2,1,0:T(8,128)(2,1)S(1)}, u32[]{:S(2)}, u32[]{:S(2)}) collective-permute-start(bf16[2,512,128]{2,1,0:T(8,128)(2,1)S(1)} %get-tuple-element.24), channel_id=1, source_target_pairs={{0,448},{32,480},{64,0},{96,32},{128,64},{160,96},{192,128},{224,1... | collective-permute-start | bytes 786440 | tf_op jit(solution)/shard_map/ppermute | solution.py:166
  225.1 3.5 %copy-start.9 = (bf16[2,512,128]{2,1,0:T(8,128)(2,1)}, bf16[2,512,128]{2,1,0:T(8,128)(2,1)S(1)}, u32[]{:S(2)}) copy-start(bf16[2,512,128]{2,1,0:T(8,128)(2,1)S(1)} %collective-permute-done.2.below2) | copy-start | bytes 786436
  228.5 0.7 copy-start.10
  228.5 0.9 copy-start.5
  228.5 1.1 copy-start.6
  258.2 30.7 %copy-start.1 = (bf16[2048,128]{1,0:T(8,128)(2,1)}, bf16[2048,128]{1,0:T(8,128)(2,1)S(1)}, u32[]{:S(2)}) copy-start(bf16[2048,128]{1,0:T(8,128)(2,1)S(1)} %all-gather) | copy-start | bytes 1572868
  258.2 30.6 %collective-permute-start.4 = (bf16[4,512,128]{2,1,0:T(8,128)(2,1)S(1)}, bf16[4,512,128]{2,1,0:T(8,128)(2,1)S(1)}, u32[]{:S(2)}, u32[]{:S(2)}) collective-permute-start(bf16[4,512,128]{2,1,0:T(8,128)(2,1)S(1)} %bitcast.14), channel_id=1, source_target_pairs={{0,32},{32,64},{64,96},{96,128},{128,160},{160,192},{192,224},{224... | collective-permute-start | bytes 1572872 | tf_op jit(solution)/shard_map/ppermute | solution.py:166
  260.2 28.7 %collective-permute-start.5 = (bf16[4,512,128]{2,1,0:T(8,128)(2,1)S(1)}, bf16[4,512,128]{2,1,0:T(8,128)(2,1)S(1)}, u32[]{:S(2)}, u32[]{:S(2)}) collective-permute-start(bf16[4,512,128]{2,1,0:T(8,128)(2,1)S(1)} %bitcast.15), channel_id=1, source_target_pairs={{0,480},{32,0},{64,32},{96,64},{128,96},{160,128},{192,160},{224,1... | collective-permute-start | bytes 1572872 | tf_op jit(solution)/shard_map/ppermute | solution.py:166
  264.8 14.5 %collective-permute-start.6 = (bf16[2,512,128]{2,1,0:T(8,128)(2,1)S(1)}, bf16[2,512,128]{2,1,0:T(8,128)(2,1)S(1)}, u32[]{:S(2)}, u32[]{:S(2)}) collective-permute-start(bf16[2,512,128]{2,1,0:T(8,128)(2,1)S(1)} %bitcast.20), channel_id=1, source_target_pairs={{0,64},{32,96},{64,128},{96,160},{128,192},{160,224},{192,256},{22... | collective-permute-start | bytes 786440 | tf_op jit(solution)/shard_map/ppermute | solution.py:166
  268.9 19.9 %collective-permute-start.7 = (bf16[2,512,128]{2,1,0:T(8,128)(2,1)S(1)}, bf16[2,512,128]{2,1,0:T(8,128)(2,1)S(1)}, u32[]{:S(2)}, u32[]{:S(2)}) collective-permute-start(bf16[2,512,128]{2,1,0:T(8,128)(2,1)S(1)} %bitcast.19), channel_id=1, source_target_pairs={{0,448},{32,480},{64,0},{96,32},{128,64},{160,96},{192,128},{224,1... | collective-permute-start | bytes 786440 | tf_op jit(solution)/shard_map/ppermute | solution.py:166
  279.3 9.6 %copy-start.11 = (bf16[2,512,128]{2,1,0:T(8,128)(2,1)}, bf16[2,512,128]{2,1,0:T(8,128)(2,1)S(1)}, u32[]{:S(2)}) copy-start(bf16[2,512,128]{2,1,0:T(8,128)(2,1)S(1)} %collective-permute-done.6.below2) | copy-start | bytes 786436
  288.8 0.7 copy-start.12
  288.8 0.9 copy-start.7
  288.8 1.1 copy-start.8
  289.9 0.8 copy-start.3

commit v2 on v1

--- a/solution.py
+++ b/solution.py
@@ -69,40 +69,30 @@
     return out
 
 
-def passed_on(pairs, sems):
-    return [pltpu.make_async_copy(src, dst, sems.at[i]) for i, (src, dst) in enumerate(pairs)]
-
-
-def block_of(w, k, r, stride, at, size):
-    per = w.shape[0] // (SUB * stride)
-    first = (k * stride + r) * per
-    return jnp.concatenate([w[first + j, at : at + size, :] for j in range(per)], axis=0)
-
-
-def gate_up_kernel(
-    res, own, below, above, below2, above2, weight, hidden, gate_out, up_out, rhs, sems, *, stride
-):
+def part_at(first, k, parts, size):
+    return pl.ds(pl.multiple_of(((first + parts - k) % parts) * size, size), size)
+
+
+def gate_up_kernel(ids, *refs, stride, parts):
+    five, weights = refs[:5], refs[5 : 5 + parts]
+    hidden, gate_out, up_out, whole, sems = refs[5 + parts :]
     rows, width = hidden.shape
-    size = weight.shape[1] // 2
-    copies = passed_on(
-        ((weight.at[:, :size, :], gate_out), (weight.at[:, size:, :], up_out)), sems
-    )
+    size = weights[0].shape[1] // 2
+    copies = []
+    for k, w in enumerate(weights):
+        at = part_at(ids[1], k, parts, size)
+        for j, dst in enumerate((gate_out, up_out)):
+            src = w.at[:, j * size : (j + 1) * size, :]
+            copies.append(pltpu.make_async_copy(src, dst.at[:, at, :], sems.at[2 * k + j]))
+            whole[:, at, j * width : (j + 1) * width] = w[:, j * size : (j + 1) * size, :]
     for c in copies:
         c.start()
-    order = pieces(own, below, above, below2, above2, res[0], stride)
-    for n, (_, _, wk, r) in enumerate(order):
-        for j in range(2):
-            half = rhs.at[n, j * (rhs.shape[1] // 2) : (j + 1) * (rhs.shape[1] // 2), :]
-            half[:, :width] = block_of(weight, wk + j, r, stride, 0, size)
-            half[:, width:] = block_of(weight, wk + j, r, stride, size, size)
+    order = pieces(*five, ids[0], stride)
     step = 128
 
     def one(i, carry):
         at = pl.ds(pl.multiple_of(i * step, step), step)
-        acc = jnp.zeros((step, 2 * width), F32)
-        for n, (ref, k, _, _) in enumerate(order):
-            lhs = jnp.concatenate([ref[k, at, :], ref[k + 1, at, :]], axis=1)
-            acc = acc + jnp.dot(lhs, rhs[n], preferred_element_type=F32)
+        acc = multiply(order, at, whole, stride)
         g = jnp.minimum(acc[:, :width], 7.0)
         u = jnp.clip(acc[:, width:], -7.0, 7.0)
         hidden[at, :] = (g * jax.nn.sigmoid(1.702 * g) * (u + 1.0)).astype(BF16)
@@ -113,27 +103,38 @@
         c.wait()
 
 
-def down_kernel(
-    res, own, below, above, below2, above2, weight, out, down_out, rhs, sems, *, stride
-):
-    rows, width = out.shape
-    copies = passed_on(((weight, down_out),), sems)
+def multiply(order, at, whole, stride):
+    per = whole.shape[0] // (SUB * stride)
+    acc = None
+    for ref, k, wk, r in order:
+        lhs = jnp.concatenate([ref[k, at, :], ref[k + 1, at, :]], axis=1)
+        rhs = jnp.concatenate(
+            [whole[((wk + j) * stride + r) * per + i] for j in range(2) for i in range(per)],
+            axis=0,
+        )
+        part = jnp.dot(lhs, rhs, preferred_element_type=F32)
+        acc = part if acc is None else acc + part
+    return acc
+
+
+def down_kernel(ids, *refs, stride, parts):
+    five, weights = refs[:5], refs[5 : 5 + parts]
+    out, down_out, whole, sems = refs[5 + parts :]
+    rows, _ = out.shape
+    size = weights[0].shape[1]
+    copies = []
+    for k, w in enumerate(weights):
+        at = part_at(ids[1], k, parts, size)
+        copies.append(pltpu.make_async_copy(w, down_out.at[:, at, :], sems.at[k]))
+        whole[:, at, :] = w[...]
     for c in copies:
         c.start()
-    order = pieces(own, below, above, below2, above2, res[0], stride)
-    for n, (_, _, wk, r) in enumerate(order):
-        for j in range(2):
-            half = rhs.at[n, j * (rhs.shape[1] // 2) : (j + 1) * (rhs.shape[1] // 2), :]
-            half[...] = block_of(weight, wk + j, r, stride, 0, weight.shape[1])
+    order = pieces(*five, ids[0], stride)
     step = 128
 
     def one(i, carry):
         at = pl.ds(pl.multiple_of(i * step, step), step)
-        acc = jnp.zeros((step, width), F32)
-        for n, (ref, k, _, _) in enumerate(order):
-            lhs = jnp.concatenate([ref[k, at, :], ref[k + 1, at, :]], axis=1)
-            acc = acc + jnp.dot(lhs, rhs[n], preferred_element_type=F32)
-        out[at, :] = acc.astype(BF16)
+        out[at, :] = multiply(order, at, whole, stride).astype(BF16)
         return carry
 
     lax.fori_loop(0, rows // step, one, 0)
@@ -166,24 +167,33 @@
         return lax.ppermute(x, "fs", [(i, (i + by) % count) for i in range(count)])
 
     half = SUB // 2
-    return (
-        own,
-        shift(own, 1),
-        shift(own, -1),
-        shift(own[:half], 2),
-        shift(own[half:], -2),
-    )
+    low, high = own[:half], own[half:]
+    return [own, shift(own, 1), shift(own, -1), shift(low, 2), shift(high, -2)]
+
+
+def other_groups(x):
+    count = lax.axis_size("grp")
+    return [x] + [
+        lax.ppermute(x, "grp", [(i, (i + k) % count) for i in range(count)])
+        for k in range(1, count)
+    ]
+
+
+def in_vmem(xs):
+    return [pltpu.with_memory_space_constraint(x, pltpu.VMEM) for x in xs]
 
 
 def body(tokens, route_expert, route_weight, norm_gain, gate_train, up_train, down_train):
     tp_count = lax.axis_size("tp")
     fs_count = lax.axis_size("fs")
     stride = fs_count // SUB
+    parts = lax.axis_size("grp")
     tok_rows, width = tokens.shape
     cols = width // fs_count
     slots = EXPERTS * CAP
     my_block = lax.axis_index("fs").astype(jnp.int32)
-    res = (my_block % stride).reshape(1)
+    my_group = lax.axis_index("grp").astype(jnp.int32)
+    ids = jnp.stack([my_block % stride, my_group])
 
     buffer, comb_hi, comb_lo = pl.pallas_call(
         prep_kernel,
@@ -194,50 +204,58 @@
             jax.ShapeDtypeStruct((slots, tok_rows), BF16),
             jax.ShapeDtypeStruct((slots, tok_rows), BF16),
         ],
+        compiler_params=pltpu.CompilerParams(vmem_limit_bytes=16 << 20),
         name="prep",
     )(my_block.reshape(1), tokens, route_expert.T, route_weight.T)
     arrived = exchange(buffer.reshape(EXPERTS, CAP, cols)).reshape(slots, cols)
 
-    gain = norm_gain[None, :, None]
+    size = gate_train.shape[1] // parts
+
+    def share(w):
+        return lax.dynamic_slice_in_dim(w, my_group * size, size, 1)
+
+    gain = lax.dynamic_slice_in_dim(norm_gain, my_group * size, size)[None, :, None]
     packed = jnp.concatenate(
-        [(gate_train * gain).astype(BF16), (up_train * gain).astype(BF16)], axis=1
+        [(share(gate_train) * gain).astype(BF16), (share(up_train) * gain).astype(BF16)], axis=1
     )
     both = exchange(after(packed, arrived))
+    down_part = exchange(after(share(down_train).astype(BF16), both))
     served = jax.ShapeDtypeStruct(down_train.shape, BF16)
     hbm = pl.BlockSpec(memory_space=pl.ANY)
-    pairs = fs_count // 2
 
     hidden, gate_serve, up_serve = pl.pallas_call(
-        functools.partial(gate_up_kernel, stride=stride),
-        in_specs=[sm()] + [vm()] * 6,
+        functools.partial(gate_up_kernel, stride=stride, parts=parts),
+        in_specs=[sm()] + [vm()] * (5 + parts),
         out_specs=[vm(), hbm, hbm],
         out_shape=[jax.ShapeDtypeStruct((slots, both.shape[2]), BF16), served, served],
         scratch_shapes=[
-            pltpu.VMEM((pairs, 2 * cols, 2 * both.shape[2]), BF16),
-            pltpu.SemaphoreType.DMA((2,)),
+            pltpu.VMEM(served.shape[:2] + (2 * both.shape[2],), BF16),
+            pltpu.SemaphoreType.DMA((2 * parts,)),
         ],
+        compiler_params=pltpu.CompilerParams(vmem_limit_bytes=16 << 20),
         name="gate_up",
-    )(res, *gather(arrived), both)
-    arrived_down = exchange(after(down_train.astype(BF16), both))
+    )(ids, *in_vmem(gather(arrived) + other_groups(both)))
     expert_out, down_serve = pl.pallas_call(
-        functools.partial(down_kernel, stride=stride),
-        in_specs=[sm()] + [vm()] * 6,
+        functools.partial(down_kernel, stride=stride, parts=parts),
+        in_specs=[sm()] + [vm()] * (5 + parts),
         out_specs=[vm(), hbm],
         out_shape=[jax.ShapeDtypeStruct((slots, down_train.shape[2]), BF16), served],
         scratch_shapes=[
-            pltpu.VMEM((pairs, 2 * both.shape[2], down_train.shape[2]), BF16),
-            pltpu.SemaphoreType.DMA((1,)),
+            pltpu.VMEM(served.shape, BF16),
+            pltpu.SemaphoreType.DMA((parts,)),
         ],
+        compiler_params=pltpu.CompilerParams(vmem_limit_bytes=16 << 20),
         name="down",
-    )(res, *gather(hidden), arrived_down)
+    )(ids, *in_vmem(gather(hidden) + other_groups(down_part)))
     returned = exchange(expert_out.reshape(tp_count, slots // tp_count, -1)).reshape(slots, -1)
     mixed = pl.pallas_call(
         combine_kernel,
         in_specs=[vm()] * 3,
         out_specs=vm(),
         out_shape=jax.ShapeDtypeStruct((tok_rows, returned.shape[1]), BF16),
+        compiler_params=pltpu.CompilerParams(vmem_limit_bytes=16 << 20),
         name="combine",
-    )(comb_hi, comb_lo, returned)
+    )(comb_hi, comb_lo, *in_vmem([returned]))
 
     def whole(w):
         return w.reshape(1, -1, w.shape[-1])

time: 329 us -> 298 us (0.906)
  the two profiles are of different devices: /device:TPU:5 before, /device:TPU:6 now
where the time goes in v2:
time: 298 us; the launch traced here: 296 us
  blocking collectives  138 us (46%)
  starting transfers between devices  77.4 us (26%)
  waiting for transfers between devices  66.3 us (22%)
  Pallas kernels  6.43 us (2%)
  local copies, waits for them, and re-layouts  4.57 us (2%)
    all_gather x2, blocking collectives, gather(): own = lax.all_gather(block, 'fs', axis=0, axis_index_groups=groups)  107 us
    all_to_all x3, waiting for transfers between devices, exchange(): return lax.all_to_all(x, 'tp', split_axis=0, concat_axis=0, tiled=True)  46.3 us
    ppermute x8, starting transfers between devices, shift(): return lax.ppermute(x, 'fs', [(i, (i + by) % count) for i in range(count)])  46 us
    all_to_all x1, blocking collectives, exchange(): return lax.all_to_all(x, 'tp', split_axis=0, concat_axis=0, tiled=True)  31 us
    all_to_all x3, starting transfers between devices, exchange(): return lax.all_to_all(x, 'tp', split_axis=0, concat_axis=0, tiled=True)  24.9 us
    ppermute x8, waiting for transfers between devices, shift(): return lax.ppermute(x, 'fs', [(i, (i + by) % count) for i in range(count)])  19.9 us
    ppermute x2, starting transfers between devices, other_groups(): lax.ppermute(x, 'grp', [(i, (i + k) % count) for i in range(count)])  6.56 us
  transfers between devices with their start and end apart: 13, of which 6 were waited for; matrix products, arithmetic and copies ran while one was open for 1% of the time, Pallas kernels for 1%

profile of v2, /device:TPU:6, one launch (start us, length us, event | category | flops | bytes accessed | tf_op | source)
XLA Modules:
  0.0 296.3 jit_solution(13458780416669396322)
XLA Ops:
  0.7 0.7 copy-done.6
  1.5 1.4 multiply_convert_fusion.1
  2.8 0.9 pad_maximum_fusion
  3.7 15.3 %all-to-all-start.1 = ((bf16[32,64,128]{2,1,0:T(8,128)(2,1)}), bf16[32,64,128]{2,1,0:T(8,128)(2,1)S(1)}, u32[]{:S(2)}, u32[]{:S(2)}) async-start(bf16[32,64,128]{2,1,0:T(8,128)(2,1)} %pad_maximum_fusion), calls=%async_computation.1 | async-start | bytes 1048576 | tf_op jit(solution)/shard_map/all_to_all | solution.py:153
  19.7 1.0 prep.1
  21.4 30.7 %all-to-all-done.1.refs_5_ = bf16[32,64,128]{2,1,0:T(8,128)(2,1)S(1)} async-done(((bf16[32,64,128]{2,1,0:T(8,128)(2,1)}), bf16[32,64,128]{2,1,0:T(8,128)(2,1)S(1)}, u32[]{:S(2)}, u32[]{:S(2)}) %all-to-all-start.1) | async-done | bytes 524320 | tf_op jit(solution)/shard_map/all_to_all | solution.py:153
  52.1 4.8 %all-to-all-start = ((bf16[32,16,128]{2,1,0:T(8,128)(2,1)}), bf16[32,16,128]{2,1,0:T(8,128)(2,1)S(1)}, u32[]{:S(2)}, u32[]{:S(2)}) async-start(bf16[32,16,128]{2,1,0:T(8,128)(2,1)} %bitcast.5), calls=%async_computation | async-start | bytes 262144 | tf_op jit(solution)/shard_map/all_to_all | solution.py:153
  56.9 0.8 dynamic-slice_convert_fusion
  57.7 15.6 %all-to-all-done = bf16[32,16,128]{2,1,0:T(8,128)(2,1)S(1)} async-done(((bf16[32,16,128]{2,1,0:T(8,128)(2,1)}), bf16[32,16,128]{2,1,0:T(8,128)(2,1)S(1)}, u32[]{:S(2)}, u32[]{:S(2)}) %all-to-all-start) | async-done | bytes 131104 | tf_op jit(solution)/shard_map/all_to_all | solution.py:153
  73.3 4.8 %all-to-all-start.2 = ((bf16[32,32,128]{2,1,0:T(8,128)(2,1)}), bf16[32,32,128]{2,1,0:T(8,128)(2,1)S(1)}, u32[]{:S(2)}, u32[]{:S(2)}) async-start(bf16[32,32,128]{2,1,0:T(8,128)(2,1)} %dynamic-slice_convert_fusion), calls=%async_computation.2 | async-start | bytes 524288 | tf_op jit(solution)/shard_map/all_to_all | solution.py:153
  78.1 83.9 %all_gather.9.refs_0_ = bf16[4,512,128]{2,1,0:T(8,128)(2,1)S(1)} all-gather(bf16[1,512,128]{2,1,0:T(8,128)(2,1)S(1)} %bitcast.22), channel_id=1, replica_groups={{0,128,256,384},{32,160,288,416},{64,192,320,448},{96,224,352,480},{1,1..., dimensions={0}, use_global_device_ids=true | all-gather | bytes 655360 | tf_op jit(solution)/shard_map/all_gather | solution.py:164
  162.0 8.0 %collective-permute-start = (bf16[4,512,128]{2,1,0:T(8,128)(2,1)S(1)}, bf16[4,512,128]{2,1,0:T(8,128)(2,1)S(1)}, u32[]{:S(2)}, u32[]{:S(2)}) collective-permute-start(bf16[4,512,128]{2,1,0:T(8,128)(2,1)S(1)} %all_gather.9.refs_0_), channel_id=1, source_target_pairs={{0,32},{32,64},{64,96},{96,128},{128,160},{160,192},{192,224},{224... | collective-permute-start | bytes 1572872 | tf_op jit(solution)/shard_map/ppermute | solution.py:167
  170.0 14.9 %collective-permute-start.1 = (bf16[4,512,128]{2,1,0:T(8,128)(2,1)S(1)}, bf16[4,512,128]{2,1,0:T(8,128)(2,1)S(1)}, u32[]{:S(2)}, u32[]{:S(2)}) collective-permute-start(bf16[4,512,128]{2,1,0:T(8,128)(2,1)S(1)} %all_gather.9.refs_0_), channel_id=1, source_target_pairs={{0,480},{32,0},{64,32},{96,64},{128,96},{160,128},{192,160},{224,1... | collective-permute-start | bytes 1572872 | tf_op jit(solution)/shard_map/ppermute | solution.py:167
  185.0 2.4 collective-permute-start.4
  187.4 0.8 fusion.1
  188.2 1.9 collective-permute-start.2
  190.1 6.1 %collective-permute-start.3 = (bf16[2,512,128]{2,1,0:T(8,128)(2,1)}, bf16[2,512,128]{2,1,0:T(8,128)(2,1)}, u32[]{:S(2)}, u32[]{:S(2)}) collective-permute-start(bf16[2,512,128]{2,1,0:T(8,128)(2,1)} %get-tuple-element.24), channel_id=1, source_target_pairs={{0,448},{32,480},{64,0},{96,32},{128,64},{160,96},{192,128},{224,1... | collective-permute-start | bytes 786440 | tf_op jit(solution)/shard_map/ppermute | solution.py:167
  196.3 7.6 %collective-permute-done.2.refs_3_ = bf16[2,512,128]{2,1,0:T(8,128)(2,1)} collective-permute-done((bf16[2,512,128]{2,1,0:T(8,128)(2,1)}, bf16[2,512,128]{2,1,0:T(8,128)(2,1)}, u32[]{:S(2)}, u32[]{:S(2)}) %collective-permute-start.2) | collective-permute-done | bytes 262176 | tf_op jit(solution)/shard_map/ppermute | solution.py:167
  203.9 0.9 collective-permute-done.3.refs_4_
  204.8 2.7 gate_up.1
  207.5 23.5 %all-gather = bf16[2048,128]{1,0:T(8,128)(2,1)S(1)} all-gather(bf16[512,128]{1,0:T(8,128)(2,1)S(1)} %get-tuple-element.16), channel_id=2, replica_groups={{0,128,256,384},{32,160,288,416},{64,192,320,448},{96,224,352,480},{1,1..., dimensions={0}, use_global_device_ids=true | all-gather | bytes 655360 | tf_op jit(solution)/shard_map/all_gather | solution.py:164
  231.1 1.9 collective-permute-start.5
  233.0 5.2 %collective-permute-start.6 = (bf16[4,512,128]{2,1,0:T(8,128)(2,1)S(1)}, bf16[4,512,128]{2,1,0:T(8,128)(2,1)S(1)}, u32[]{:S(2)}, u32[]{:S(2)}) collective-permute-start(bf16[4,512,128]{2,1,0:T(8,128)(2,1)S(1)} %bitcast.16), channel_id=1, source_target_pairs={{0,480},{32,0},{64,32},{96,64},{128,96},{160,128},{192,160},{224,1... | collective-permute-start | bytes 1572872 | tf_op jit(solution)/shard_map/ppermute | solution.py:167
  238.2 0.8 fusion
  239.0 3.8 %collective-permute-start.7 = (bf16[2,512,128]{2,1,0:T(8,128)(2,1)}, bf16[2,512,128]{2,1,0:T(8,128)(2,1)S(1)}, u32[]{:S(2)}, u32[]{:S(2)}) collective-permute-start(bf16[2,512,128]{2,1,0:T(8,128)(2,1)} %bitcast.10), channel_id=1, source_target_pairs={{0,64},{32,96},{64,128},{96,160},{128,192},{160,224},{192,256},{22... | collective-permute-start | bytes 786440 | tf_op jit(solution)/shard_map/ppermute | solution.py:167
  242.9 4.2 %collective-permute-start.8 = (bf16[2,512,128]{2,1,0:T(8,128)(2,1)}, bf16[2,512,128]{2,1,0:T(8,128)(2,1)S(1)}, u32[]{:S(2)}, u32[]{:S(2)}) collective-permute-start(bf16[2,512,128]{2,1,0:T(8,128)(2,1)} %bitcast.11), channel_id=1, source_target_pairs={{0,448},{32,480},{64,0},{96,32},{128,64},{160,96},{192,128},{224,1... | collective-permute-start | bytes 786440 | tf_op jit(solution)/shard_map/ppermute | solution.py:167
  247.0 4.2 %collective-permute-start.9 = (bf16[32,32,128]{2,1,0:T(8,128)(2,1)S(1)}, bf16[32,32,128]{2,1,0:T(8,128)(2,1)S(1)}, u32[]{:S(2)}, u32[]{:S(2)}) collective-permute-start(bf16[32,32,128]{2,1,0:T(8,128)(2,1)S(1)} %all-to-all-done.2.refs_5_), channel_id=1, source_target_pairs={{0,512},{512,0},{1,513},{513,1},{2,514},{514,2},{3,515},{515,3},{4... | collective-permute-start | bytes 786440 | tf_op jit(solution)/shard_map/ppermute | solution.py:177
  251.2 3.1 %collective-permute-done.7.refs_3_ = bf16[2,512,128]{2,1,0:T(8,128)(2,1)S(1)} collective-permute-done((bf16[2,512,128]{2,1,0:T(8,128)(2,1)}, bf16[2,512,128]{2,1,0:T(8,128)(2,1)S(1)}, u32[]{:S(2)}, u32[]{:S(2)}) %collective-permute-start.7) | collective-permute-done | bytes 262176 | tf_op jit(solution)/shard_map/ppermute | solution.py:167
  254.3 8.4 %collective-permute-done.8.refs_4_ = bf16[2,512,128]{2,1,0:T(8,128)(2,1)S(1)} collective-permute-done((bf16[2,512,128]{2,1,0:T(8,128)(2,1)}, bf16[2,512,128]{2,1,0:T(8,128)(2,1)S(1)}, u32[]{:S(2)}, u32[]{:S(2)}) %collective-permute-start.8) | collective-permute-done | bytes 262176 | tf_op jit(solution)/shard_map/ppermute | solution.py:167
  262.7 1.8 down.1
  264.5 31.0 %all_to_all.20 = bf16[32,16,128]{2,1,0:T(8,128)(2,1)S(1)} all-to-all(bf16[32,16,128]{2,1,0:T(8,128)(2,1)S(1)} %bitcast.19), channel_id=1, replica_groups=mesh['grp'=2,'fs'=16,'tp'=32] {'tp'}, dimensions={0} | all-to-all | bytes 262144 | tf_op jit(solution)/shard_map/all_to_all | solution.py:153
  295.4 0.9 combine.1
  (22 shorter events, 1.5 us)
Async XLA Ops:
  0.6 56.3 %copy-start = (f32[32,64,128]{2,1,0:T(8,128)S(1)}, f32[32,64,128]{2,1,0:T(8,128)}, u32[]{:S(2)}) copy-start(f32[32,64,128]{2,1,0:T(8,128)} %param.13) | copy-start | bytes 3145732
  0.7 0.7 copy-start.6
  3.7 15.3 %copy-start.1 = (bf16[120,2048]{1,0:T(8,128)(2,1)S(1)}, bf16[120,2048]{1,0:T(8,128)(2,1)}, u32[]{:S(2)}) copy-start(bf16[120,2048]{1,0:T(8,128)(2,1)} %tokens.1) | copy-start | bytes 1474564
  3.7 48.4 %all-to-all-start.1 = ((bf16[32,64,128]{2,1,0:T(8,128)(2,1)}), bf16[32,64,128]{2,1,0:T(8,128)(2,1)S(1)}, u32[]{:S(2)}, u32[]{:S(2)}) async-start(bf16[32,64,128]{2,1,0:T(8,128)(2,1)} %pad_maximum_fusion), calls=%async_computation.1 | async-start | bytes 1048576 | tf_op jit(solution)/shard_map/all_to_all | solution.py:153
  19.0 0.7 copy-start.5
  19.0 0.7 copy-start.4
  20.8 0.6 copy-start.2
  52.1 21.2 %all-to-all-start = ((bf16[32,16,128]{2,1,0:T(8,128)(2,1)}), bf16[32,16,128]{2,1,0:T(8,128)(2,1)S(1)}, u32[]{:S(2)}, u32[]{:S(2)}) async-start(bf16[32,16,128]{2,1,0:T(8,128)(2,1)} %bitcast.5), calls=%async_computation | async-start | bytes 262144 | tf_op jit(solution)/shard_map/all_to_all | solution.py:153
  73.3 173.8 %all-to-all-start.2 = ((bf16[32,32,128]{2,1,0:T(8,128)(2,1)}), bf16[32,32,128]{2,1,0:T(8,128)(2,1)S(1)}, u32[]{:S(2)}, u32[]{:S(2)}) async-start(bf16[32,32,128]{2,1,0:T(8,128)(2,1)} %dynamic-slice_convert_fusion), calls=%async_computation.2 | async-start | bytes 524288 | tf_op jit(solution)/shard_map/all_to_all | solution.py:153
  162.0 42.8 %collective-permute-start = (bf16[4,512,128]{2,1,0:T(8,128)(2,1)S(1)}, bf16[4,512,128]{2,1,0:T(8,128)(2,1)S(1)}, u32[]{:S(2)}, u32[]{:S(2)}) collective-permute-start(bf16[4,512,128]{2,1,0:T(8,128)(2,1)S(1)} %all_gather.9.refs_0_), channel_id=1, source_target_pairs={{0,32},{32,64},{64,96},{96,128},{128,160},{160,192},{192,224},{224... | collective-permute-start | bytes 1572872 | tf_op jit(solution)/shard_map/ppermute | solution.py:167
  170.0 34.8 %collective-permute-start.1 = (bf16[4,512,128]{2,1,0:T(8,128)(2,1)S(1)}, bf16[4,512,128]{2,1,0:T(8,128)(2,1)S(1)}, u32[]{:S(2)}, u32[]{:S(2)}) collective-permute-start(bf16[4,512,128]{2,1,0:T(8,128)(2,1)S(1)} %all_gather.9.refs_0_), channel_id=1, source_target_pairs={{0,480},{32,0},{64,32},{96,64},{128,96},{160,128},{192,160},{224,1... | collective-permute-start | bytes 1572872 | tf_op jit(solution)/shard_map/ppermute | solution.py:167
  185.0 19.8 %collective-permute-start.4 = (bf16[32,64,128]{2,1,0:T(8,128)(2,1)S(1)}, bf16[32,64,128]{2,1,0:T(8,128)(2,1)}, u32[]{:S(2)}, u32[]{:S(2)}) collective-permute-start(bf16[32,64,128]{2,1,0:T(8,128)(2,1)S(1)} %all-to-all-done.1.refs_5_), channel_id=1, source_target_pairs={{0,512},{512,0},{1,513},{513,1},{2,514},{514,2},{3,515},{515,3},{4... | collective-permute-start | bytes 1572872 | tf_op jit(solution)/shard_map/ppermute | solution.py:177
  188.2 15.7 %collective-permute-start.2 = (bf16[2,512,128]{2,1,0:T(8,128)(2,1)}, bf16[2,512,128]{2,1,0:T(8,128)(2,1)}, u32[]{:S(2)}, u32[]{:S(2)}) collective-permute-start(bf16[2,512,128]{2,1,0:T(8,128)(2,1)} %get-tuple-element.25), channel_id=1, source_target_pairs={{0,64},{32,96},{64,128},{96,160},{128,192},{160,224},{192,256},{22... | collective-permute-start | bytes 786440 | tf_op jit(solution)/shard_map/ppermute | solution.py:167
  190.1 14.6 %collective-permute-start.3 = (bf16[2,512,128]{2,1,0:T(8,128)(2,1)}, bf16[2,512,128]{2,1,0:T(8,128)(2,1)}, u32[]{:S(2)}, u32[]{:S(2)}) collective-permute-start(bf16[2,512,128]{2,1,0:T(8,128)(2,1)} %get-tuple-element.24), channel_id=1, source_target_pairs={{0,448},{32,480},{64,0},{96,32},{128,64},{160,96},{192,128},{224,1... | collective-permute-start | bytes 786440 | tf_op jit(solution)/shard_map/ppermute | solution.py:167
  231.1 31.6 %collective-permute-start.5 = (bf16[4,512,128]{2,1,0:T(8,128)(2,1)S(1)}, bf16[4,512,128]{2,1,0:T(8,128)(2,1)S(1)}, u32[]{:S(2)}, u32[]{:S(2)}) collective-permute-start(bf16[4,512,128]{2,1,0:T(8,128)(2,1)S(1)} %bitcast.15), channel_id=1, source_target_pairs={{0,32},{32,64},{64,96},{96,128},{128,160},{160,192},{192,224},{224... | collective-permute-start | bytes 1572872 | tf_op jit(solution)/shard_map/ppermute | solution.py:167
  233.0 29.6 %collective-permute-start.6 = (bf16[4,512,128]{2,1,0:T(8,128)(2,1)S(1)}, bf16[4,512,128]{2,1,0:T(8,128)(2,1)S(1)}, u32[]{:S(2)}, u32[]{:S(2)}) collective-permute-start(bf16[4,512,128]{2,1,0:T(8,128)(2,1)S(1)} %bitcast.16), channel_id=1, source_target_pairs={{0,480},{32,0},{64,32},{96,64},{128,96},{160,128},{192,160},{224,1... | collective-permute-start | bytes 1572872 | tf_op jit(solution)/shard_map/ppermute | solution.py:167
  239.0 15.2 %collective-permute-start.7 = (bf16[2,512,128]{2,1,0:T(8,128)(2,1)}, bf16[2,512,128]{2,1,0:T(8,128)(2,1)S(1)}, u32[]{:S(2)}, u32[]{:S(2)}) collective-permute-start(bf16[2,512,128]{2,1,0:T(8,128)(2,1)} %bitcast.10), channel_id=1, source_target_pairs={{0,64},{32,96},{64,128},{96,160},{128,192},{160,224},{192,256},{22... | collective-permute-start | bytes 786440 | tf_op jit(solution)/shard_map/ppermute | solution.py:167
  242.9 19.8 %collective-permute-start.8 = (bf16[2,512,128]{2,1,0:T(8,128)(2,1)}, bf16[2,512,128]{2,1,0:T(8,128)(2,1)S(1)}, u32[]{:S(2)}, u32[]{:S(2)}) collective-permute-start(bf16[2,512,128]{2,1,0:T(8,128)(2,1)} %bitcast.11), channel_id=1, source_target_pairs={{0,448},{32,480},{64,0},{96,32},{128,64},{160,96},{192,128},{224,1... | collective-permute-start | bytes 786440 | tf_op jit(solution)/shard_map/ppermute | solution.py:167
  247.0 15.6 %collective-permute-start.9 = (bf16[32,32,128]{2,1,0:T(8,128)(2,1)S(1)}, bf16[32,32,128]{2,1,0:T(8,128)(2,1)S(1)}, u32[]{:S(2)}, u32[]{:S(2)}) collective-permute-start(bf16[32,32,128]{2,1,0:T(8,128)(2,1)S(1)} %all-to-all-done.2.refs_5_), channel_id=1, source_target_pairs={{0,512},{512,0},{1,513},{513,1},{2,514},{514,2},{3,515},{515,3},{4... | collective-permute-start | bytes 786440 | tf_op jit(solution)/shard_map/ppermute | solution.py:177
  264.4 31.0 %copy-start.3 = (bf16[512,120]{1,0:T(8,128)(2,1)S(1)}, bf16[512,120]{1,0:T(8,128)(2,1)}, u32[]{:S(2)}) copy-start(bf16[512,120]{1,0:T(8,128)(2,1)} %copy-done.2) | copy-start | bytes 368644

commit v3 on v2

--- a/solution.py
+++ b/solution.py
@@ -57,15 +57,16 @@
     comb_lo[...] = (comb - high.astype(F32)).astype(BF16)
 
 
-def pieces(own, below, above, below2, above2, res, stride):
+def pieces(own, first, second, low, high, res, stride):
     half = SUB // 2
+    side = (res + 1 + 2 * (1 - res % 2)) % stride
     out = []
-    for ref, r in ((own, res), (below, (res + stride - 1) % stride), (above, (res + 1) % stride)):
+    for ref, r in ((own, res), (first, res + 1 - 2 * (res % 2)), (second, side)):
         for k in range(0, SUB, 2):
             out.append((ref, k, k, r))
     for k in range(0, half, 2):
-        out.append((below2, k, k, (res + 2) % stride))
-        out.append((above2, k, half + k, (res + 2) % stride))
+        out.append((low, k, k, (res + 2) % stride))
+        out.append((high, k, half + k, (res + 2) % stride))
     return out
 
 
@@ -163,12 +164,18 @@
     groups = [[i + stride * j for j in range(SUB)] for i in range(stride)]
     own = lax.all_gather(block, "fs", axis=0, axis_index_groups=groups)
 
-    def shift(x, by):
-        return lax.ppermute(x, "fs", [(i, (i + by) % count) for i in range(count)])
+    def swap(x, partner):
+        return lax.ppermute(x, "fs", [(i, partner(i) % count) for i in range(count)])
 
     half = SUB // 2
     low, high = own[:half], own[half:]
-    return [own, shift(own, 1), shift(own, -1), shift(low, 2), shift(high, -2)]
+    return [
+        own,
+        swap(own, lambda i: i ^ 1),
+        swap(own, lambda i: i + 1 if i & 1 else i - 1),
+        swap(low, lambda i: i ^ 2),
+        swap(high, lambda i: i + 2 if i & 2 else i - 2),
+    ]
 
 
 def other_groups(x):
@@ -204,7 +211,6 @@
             jax.ShapeDtypeStruct((slots, tok_rows), BF16),
             jax.ShapeDtypeStruct((slots, tok_rows), BF16),
         ],
-        compiler_params=pltpu.CompilerParams(vmem_limit_bytes=16 << 20),
         name="prep",
     )(my_block.reshape(1), tokens, route_expert.T, route_weight.T)
     arrived = exchange(buffer.reshape(EXPERTS, CAP, cols)).reshape(slots, cols)

time: 298 us -> 296 us (level)
  blocking collectives: 138 us -> 144 us
  starting transfers between devices: 77.4 us -> 73.5 us
  waiting for transfers between devices: 66.3 us -> 62.9 us
    ppermute x8, waiting for transfers between devices: 19.9 us -> 16.2 us  [swap(): lax.ppermute(x, 'fs', [(i, partner(i) % count) for i in range(count)])]
  transfers between devices with their start and end apart: 13 -> 13, of which waited for: 6 -> 5; matrix products, arithmetic and copies ran while one was open for 1% -> 1% of each run, Pallas kernels for 1% -> 2%
where the time goes in v3:
time: 296 us; the launch traced here: 294 us
  blocking collectives  144 us (49%)
  starting transfers between devices  73.5 us (25%)
  waiting for transfers between devices  62.9 us (21%)
  Pallas kernels  7.48 us (3%)
  local copies, waits for them, and re-layouts  3.22 us (1%)
    all_gather x2, blocking collectives, gather(): own = lax.all_gather(block, 'fs', axis=0, axis_index_groups=groups)  110 us
    all_to_all x3, waiting for transfers between devices, exchange(): return lax.all_to_all(x, 'tp', split_axis=0, concat_axis=0, tiled=True)  46.6 us
    ppermute x8, starting transfers between devices, swap(): lax.ppermute(x, 'fs', [(i, partner(i) % count) for i in range(count)])  43.1 us
    all_to_all x1, blocking collectives, exchange(): return lax.all_to_all(x, 'tp', split_axis=0, concat_axis=0, tiled=True)  33.6 us
    all_to_all x3, starting transfers between devices, exchange(): return lax.all_to_all(x, 'tp', split_axis=0, concat_axis=0, tiled=True)  24.7 us
    ppermute x8, waiting for transfers between devices, swap(): lax.ppermute(x, 'fs', [(i, partner(i) % count) for i in range(count)])  16.2 us
  transfers between devices with their start and end apart: 13, of which 5 were waited for; matrix products, arithmetic and copies ran while one was open for 1% of the time, Pallas kernels for 2%

profile of v3, /device:TPU:6, one launch (start us, length us, event | category | flops | bytes accessed | tf_op | source)
XLA Modules:
  0.0 294.0 jit_solution(3620531435454492370)
XLA Ops:
  0.7 0.7 copy-done.3
  1.4 0.1 dynamic_slice.13
  1.5 1.4 multiply_convert_fusion.1
  2.8 0.9 pad_maximum_fusion
  3.7 15.2 %all-to-all-start.1 = ((bf16[32,64,128]{2,1,0:T(8,128)(2,1)}), bf16[32,64,128]{2,1,0:T(8,128)(2,1)S(1)}, u32[]{:S(2)}, u32[]{:S(2)}) async-start(bf16[32,64,128]{2,1,0:T(8,128)(2,1)} %pad_maximum_fusion), calls=%async_computation.1 | async-start | bytes 1048576 | tf_op jit(solution)/shard_map/all_to_all | solution.py:154
  18.9 2.1 prep.1
  21.0 31.0 %all-to-all-done.1.refs_5_ = bf16[32,64,128]{2,1,0:T(8,128)(2,1)S(1)} async-done(((bf16[32,64,128]{2,1,0:T(8,128)(2,1)}), bf16[32,64,128]{2,1,0:T(8,128)(2,1)S(1)}, u32[]{:S(2)}, u32[]{:S(2)}) %all-to-all-start.1) | async-done | bytes 524320 | tf_op jit(solution)/shard_map/all_to_all | solution.py:154
  52.0 4.8 %all-to-all-start = ((bf16[32,16,128]{2,1,0:T(8,128)(2,1)}), bf16[32,16,128]{2,1,0:T(8,128)(2,1)S(1)}, u32[]{:S(2)}, u32[]{:S(2)}) async-start(bf16[32,16,128]{2,1,0:T(8,128)(2,1)} %bitcast.21), calls=%async_computation | async-start | bytes 262144 | tf_op jit(solution)/shard_map/all_to_all | solution.py:154
  56.8 0.7 dynamic-slice_convert_fusion
  57.5 15.6 %all-to-all-done = bf16[32,16,128]{2,1,0:T(8,128)(2,1)S(1)} async-done(((bf16[32,16,128]{2,1,0:T(8,128)(2,1)}), bf16[32,16,128]{2,1,0:T(8,128)(2,1)S(1)}, u32[]{:S(2)}, u32[]{:S(2)}) %all-to-all-start) | async-done | bytes 131104 | tf_op jit(solution)/shard_map/all_to_all | solution.py:154
  73.1 4.8 %all-to-all-start.2 = ((bf16[32,32,128]{2,1,0:T(8,128)(2,1)}), bf16[32,32,128]{2,1,0:T(8,128)(2,1)S(1)}, u32[]{:S(2)}, u32[]{:S(2)}) async-start(bf16[32,32,128]{2,1,0:T(8,128)(2,1)} %dynamic-slice_convert_fusion), calls=%async_computation.2 | async-start | bytes 524288 | tf_op jit(solution)/shard_map/all_to_all | solution.py:154
  77.9 83.9 %all_gather.9.refs_0_ = bf16[4,512,128]{2,1,0:T(8,128)(2,1)S(1)} all-gather(bf16[1,512,128]{2,1,0:T(8,128)(2,1)S(1)} %bitcast.20), channel_id=1, replica_groups={{0,128,256,384},{32,160,288,416},{64,192,320,448},{96,224,352,480},{1,1..., dimensions={0}, use_global_device_ids=true | all-gather | bytes 655360 | tf_op jit(solution)/shard_map/all_gather | solution.py:165
  161.9 8.0 %collective-permute-start = (bf16[4,512,128]{2,1,0:T(8,128)(2,1)S(1)}, bf16[4,512,128]{2,1,0:T(8,128)(2,1)S(1)}, u32[]{:S(2)}, u32[]{:S(2)}) collective-permute-start(bf16[4,512,128]{2,1,0:T(8,128)(2,1)S(1)} %all_gather.9.refs_0_), channel_id=1, source_target_pairs={{0,32},{32,0},{64,96},{96,64},{128,160},{160,128},{192,224},{224,1... | collective-permute-start | bytes 1572872 | tf_op jit(solution)/shard_map/ppermute | solution.py:168
  169.9 15.0 %collective-permute-start.1 = (bf16[4,512,128]{2,1,0:T(8,128)(2,1)S(1)}, bf16[4,512,128]{2,1,0:T(8,128)(2,1)S(1)}, u32[]{:S(2)}, u32[]{:S(2)}) collective-permute-start(bf16[4,512,128]{2,1,0:T(8,128)(2,1)S(1)} %all_gather.9.refs_0_), channel_id=1, source_target_pairs={{0,480},{32,64},{64,32},{96,128},{128,96},{160,192},{192,160},{224... | collective-permute-start | bytes 1572872 | tf_op jit(solution)/shard_map/ppermute | solution.py:168
  184.9 2.4 collective-permute-start.4
  187.3 0.8 fusion.1
  188.1 1.9 collective-permute-start.2
  190.1 3.5 %collective-permute-start.3 = (bf16[2,512,128]{2,1,0:T(8,128)(2,1)}, bf16[2,512,128]{2,1,0:T(8,128)(2,1)}, u32[]{:S(2)}, u32[]{:S(2)}) collective-permute-start(bf16[2,512,128]{2,1,0:T(8,128)(2,1)} %get-tuple-element.24), channel_id=1, source_target_pairs={{0,448},{32,480},{64,128},{96,160},{128,64},{160,96},{192,256},{22... | collective-permute-start | bytes 786440 | tf_op jit(solution)/shard_map/ppermute | solution.py:168
  193.6 0.1 pad_add_fusion.ids
  193.6 10.7 %collective-permute-done.2.refs_3_ = bf16[2,512,128]{2,1,0:T(8,128)(2,1)} collective-permute-done((bf16[2,512,128]{2,1,0:T(8,128)(2,1)}, bf16[2,512,128]{2,1,0:T(8,128)(2,1)}, u32[]{:S(2)}, u32[]{:S(2)}) %collective-permute-start.2) | collective-permute-done | bytes 262176 | tf_op jit(solution)/shard_map/ppermute | solution.py:168
  204.4 2.7 gate_up.1
  207.1 26.3 %all-gather = bf16[2048,128]{1,0:T(8,128)(2,1)S(1)} all-gather(bf16[512,128]{1,0:T(8,128)(2,1)S(1)} %get-tuple-element.16), channel_id=2, replica_groups={{0,128,256,384},{32,160,288,416},{64,192,320,448},{96,224,352,480},{1,1..., dimensions={0}, use_global_device_ids=true | all-gather | bytes 655360 | tf_op jit(solution)/shard_map/all_gather | solution.py:165
  233.4 1.9 collective-permute-start.5
  235.4 2.8 collective-permute-start.6
  238.1 0.8 fusion
  238.9 4.8 %collective-permute-start.7 = (bf16[2,512,128]{2,1,0:T(8,128)(2,1)}, bf16[2,512,128]{2,1,0:T(8,128)(2,1)S(1)}, u32[]{:S(2)}, u32[]{:S(2)}) collective-permute-start(bf16[2,512,128]{2,1,0:T(8,128)(2,1)} %bitcast.10), channel_id=1, source_target_pairs={{0,64},{32,96},{64,0},{96,32},{128,192},{160,224},{192,128},{224,1... | collective-permute-start | bytes 786440 | tf_op jit(solution)/shard_map/ppermute | solution.py:168
  243.8 5.2 %collective-permute-start.8 = (bf16[2,512,128]{2,1,0:T(8,128)(2,1)}, bf16[2,512,128]{2,1,0:T(8,128)(2,1)S(1)}, u32[]{:S(2)}, u32[]{:S(2)}) collective-permute-start(bf16[2,512,128]{2,1,0:T(8,128)(2,1)} %bitcast.11), channel_id=1, source_target_pairs={{0,448},{32,480},{64,128},{96,160},{128,64},{160,96},{192,256},{22... | collective-permute-start | bytes 786440 | tf_op jit(solution)/shard_map/ppermute | solution.py:168
  249.0 3.2 %collective-permute-start.9 = (bf16[32,32,128]{2,1,0:T(8,128)(2,1)S(1)}, bf16[32,32,128]{2,1,0:T(8,128)(2,1)S(1)}, u32[]{:S(2)}, u32[]{:S(2)}) collective-permute-start(bf16[32,32,128]{2,1,0:T(8,128)(2,1)S(1)} %all-to-all-done.2.refs_5_), channel_id=1, source_target_pairs={{0,512},{512,0},{1,513},{513,1},{2,514},{514,2},{3,515},{515,3},{4... | collective-permute-start | bytes 786440 | tf_op jit(solution)/shard_map/ppermute | solution.py:184
  252.2 5.5 %collective-permute-done.7.refs_3_ = bf16[2,512,128]{2,1,0:T(8,128)(2,1)S(1)} collective-permute-done((bf16[2,512,128]{2,1,0:T(8,128)(2,1)}, bf16[2,512,128]{2,1,0:T(8,128)(2,1)S(1)}, u32[]{:S(2)}, u32[]{:S(2)}) %collective-permute-start.7) | collective-permute-done | bytes 262176 | tf_op jit(solution)/shard_map/ppermute | solution.py:168
  257.8 1.8 down.1
  259.6 33.6 %all_to_all.20 = bf16[32,16,128]{2,1,0:T(8,128)(2,1)S(1)} all-to-all(bf16[32,16,128]{2,1,0:T(8,128)(2,1)S(1)} %bitcast.19), channel_id=1, replica_groups=mesh['grp'=2,'fs'=16,'tp'=32] {'tp'}, dimensions={0} | all-to-all | bytes 262144 | tf_op jit(solution)/shard_map/all_to_all | solution.py:154
  293.2 0.9 combine.1
  (16 shorter events, 0.1 us)
Async XLA Ops:
  0.6 56.1 %copy-start = (f32[32,64,128]{2,1,0:T(8,128)S(1)}, f32[32,64,128]{2,1,0:T(8,128)}, u32[]{:S(2)}) copy-start(f32[32,64,128]{2,1,0:T(8,128)} %param.13) | copy-start | bytes 3145732
  0.7 0.7 copy-start.3
  3.7 48.3 %all-to-all-start.1 = ((bf16[32,64,128]{2,1,0:T(8,128)(2,1)}), bf16[32,64,128]{2,1,0:T(8,128)(2,1)S(1)}, u32[]{:S(2)}, u32[]{:S(2)}) async-start(bf16[32,64,128]{2,1,0:T(8,128)(2,1)} %pad_maximum_fusion), calls=%async_computation.1 | async-start | bytes 1048576 | tf_op jit(solution)/shard_map/all_to_all | solution.py:154
  52.0 21.2 %all-to-all-start = ((bf16[32,16,128]{2,1,0:T(8,128)(2,1)}), bf16[32,16,128]{2,1,0:T(8,128)(2,1)S(1)}, u32[]{:S(2)}, u32[]{:S(2)}) async-start(bf16[32,16,128]{2,1,0:T(8,128)(2,1)} %bitcast.21), calls=%async_computation | async-start | bytes 262144 | tf_op jit(solution)/shard_map/all_to_all | solution.py:154
  73.1 175.8 %all-to-all-start.2 = ((bf16[32,32,128]{2,1,0:T(8,128)(2,1)}), bf16[32,32,128]{2,1,0:T(8,128)(2,1)S(1)}, u32[]{:S(2)}, u32[]{:S(2)}) async-start(bf16[32,32,128]{2,1,0:T(8,128)(2,1)} %dynamic-slice_convert_fusion), calls=%async_computation.2 | async-start | bytes 524288 | tf_op jit(solution)/shard_map/all_to_all | solution.py:154
  161.9 42.5 %collective-permute-start = (bf16[4,512,128]{2,1,0:T(8,128)(2,1)S(1)}, bf16[4,512,128]{2,1,0:T(8,128)(2,1)S(1)}, u32[]{:S(2)}, u32[]{:S(2)}) collective-permute-start(bf16[4,512,128]{2,1,0:T(8,128)(2,1)S(1)} %all_gather.9.refs_0_), channel_id=1, source_target_pairs={{0,32},{32,0},{64,96},{96,64},{128,160},{160,128},{192,224},{224,1... | collective-permute-start | bytes 1572872 | tf_op jit(solution)/shard_map/ppermute | solution.py:168
  169.9 34.4 %collective-permute-start.1 = (bf16[4,512,128]{2,1,0:T(8,128)(2,1)S(1)}, bf16[4,512,128]{2,1,0:T(8,128)(2,1)S(1)}, u32[]{:S(2)}, u32[]{:S(2)}) collective-permute-start(bf16[4,512,128]{2,1,0:T(8,128)(2,1)S(1)} %all_gather.9.refs_0_), channel_id=1, source_target_pairs={{0,480},{32,64},{64,32},{96,128},{128,96},{160,192},{192,160},{224... | collective-permute-start | bytes 1572872 | tf_op jit(solution)/shard_map/ppermute | solution.py:168
  184.9 19.5 %collective-permute-start.4 = (bf16[32,64,128]{2,1,0:T(8,128)(2,1)S(1)}, bf16[32,64,128]{2,1,0:T(8,128)(2,1)}, u32[]{:S(2)}, u32[]{:S(2)}) collective-permute-start(bf16[32,64,128]{2,1,0:T(8,128)(2,1)S(1)} %all-to-all-done.1.refs_5_), channel_id=1, source_target_pairs={{0,512},{512,0},{1,513},{513,1},{2,514},{514,2},{3,515},{515,3},{4... | collective-permute-start | bytes 1572872 | tf_op jit(solution)/shard_map/ppermute | solution.py:184
  188.1 16.2 %collective-permute-start.2 = (bf16[2,512,128]{2,1,0:T(8,128)(2,1)}, bf16[2,512,128]{2,1,0:T(8,128)(2,1)}, u32[]{:S(2)}, u32[]{:S(2)}) collective-permute-start(bf16[2,512,128]{2,1,0:T(8,128)(2,1)} %get-tuple-element.25), channel_id=1, source_target_pairs={{0,64},{32,96},{64,0},{96,32},{128,192},{160,224},{192,128},{224,1... | collective-permute-start | bytes 786440 | tf_op jit(solution)/shard_map/ppermute | solution.py:168
  190.1 14.3 %collective-permute-start.3 = (bf16[2,512,128]{2,1,0:T(8,128)(2,1)}, bf16[2,512,128]{2,1,0:T(8,128)(2,1)}, u32[]{:S(2)}, u32[]{:S(2)}) collective-permute-start(bf16[2,512,128]{2,1,0:T(8,128)(2,1)} %get-tuple-element.24), channel_id=1, source_target_pairs={{0,448},{32,480},{64,128},{96,160},{128,64},{160,96},{192,256},{22... | collective-permute-start | bytes 786440 | tf_op jit(solution)/shard_map/ppermute | solution.py:168
  233.4 24.4 %collective-permute-start.5 = (bf16[4,512,128]{2,1,0:T(8,128)(2,1)S(1)}, bf16[4,512,128]{2,1,0:T(8,128)(2,1)S(1)}, u32[]{:S(2)}, u32[]{:S(2)}) collective-permute-start(bf16[4,512,128]{2,1,0:T(8,128)(2,1)S(1)} %bitcast.15), channel_id=1, source_target_pairs={{0,32},{32,0},{64,96},{96,64},{128,160},{160,128},{192,224},{224,1... | collective-permute-start | bytes 1572872 | tf_op jit(solution)/shard_map/ppermute | solution.py:168
  235.4 22.4 %collective-permute-start.6 = (bf16[4,512,128]{2,1,0:T(8,128)(2,1)S(1)}, bf16[4,512,128]{2,1,0:T(8,128)(2,1)S(1)}, u32[]{:S(2)}, u32[]{:S(2)}) collective-permute-start(bf16[4,512,128]{2,1,0:T(8,128)(2,1)S(1)} %bitcast.16), channel_id=1, source_target_pairs={{0,480},{32,64},{64,32},{96,128},{128,96},{160,192},{192,160},{224... | collective-permute-start | bytes 1572872 | tf_op jit(solution)/shard_map/ppermute | solution.py:168
  238.9 18.8 %collective-permute-start.7 = (bf16[2,512,128]{2,1,0:T(8,128)(2,1)}, bf16[2,512,128]{2,1,0:T(8,128)(2,1)S(1)}, u32[]{:S(2)}, u32[]{:S(2)}) collective-permute-start(bf16[2,512,128]{2,1,0:T(8,128)(2,1)} %bitcast.10), channel_id=1, source_target_pairs={{0,64},{32,96},{64,0},{96,32},{128,192},{160,224},{192,128},{224,1... | collective-permute-start | bytes 786440 | tf_op jit(solution)/shard_map/ppermute | solution.py:168
  243.8 14.0 %collective-permute-start.8 = (bf16[2,512,128]{2,1,0:T(8,128)(2,1)}, bf16[2,512,128]{2,1,0:T(8,128)(2,1)S(1)}, u32[]{:S(2)}, u32[]{:S(2)}) collective-permute-start(bf16[2,512,128]{2,1,0:T(8,128)(2,1)} %bitcast.11), channel_id=1, source_target_pairs={{0,448},{32,480},{64,128},{96,160},{128,64},{160,96},{192,256},{22... | collective-permute-start | bytes 786440 | tf_op jit(solution)/shard_map/ppermute | solution.py:168
  249.0 8.8 %collective-permute-start.9 = (bf16[32,32,128]{2,1,0:T(8,128)(2,1)S(1)}, bf16[32,32,128]{2,1,0:T(8,128)(2,1)S(1)}, u32[]{:S(2)}, u32[]{:S(2)}) collective-permute-start(bf16[32,32,128]{2,1,0:T(8,128)(2,1)S(1)} %all-to-all-done.2.refs_5_), channel_id=1, source_target_pairs={{0,512},{512,0},{1,513},{513,1},{2,514},{514,2},{3,515},{515,3},{4... | collective-permute-start | bytes 786440 | tf_op jit(solution)/shard_map/ppermute | solution.py:184
  259.6 33.6 %copy-start.1 = (bf16[512,120]{1,0:T(8,128)(2,1)S(1)}, bf16[512,120]{1,0:T(8,128)(2,1)}, u32[]{:S(2)}) copy-start(bf16[512,120]{1,0:T(8,128)(2,1)} %get-tuple-element.19.comb_hi) | copy-start | bytes 368644
  259.6 33.6 %copy-start.2 = (bf16[512,120]{1,0:T(8,128)(2,1)S(1)}, bf16[512,120]{1,0:T(8,128)(2,1)}, u32[]{:S(2)}) copy-start(bf16[512,120]{1,0:T(8,128)(2,1)} %get-tuple-element.20.comb_lo) | copy-start | bytes 368644

commit v4 on v3

--- a/solution.py
+++ b/solution.py
@@ -24,20 +24,12 @@
     return pl.BlockSpec(memory_space=pltpu.SMEM)
 
 
-def prep_kernel(block, tokens, route_t, weight_t, buffer, comb_hi, comb_lo):
-    rows, _ = tokens.shape
-    floated = tokens[...].astype(F32)
-    inv = lax.rsqrt(jnp.mean(floated * floated, axis=-1, keepdims=True) + 1e-06)
-    cols = buffer.shape[1]
-    part = tokens[:, pl.ds(pl.multiple_of(block[0] * cols, cols), cols)].astype(F32)
-    normed = (part * inv).astype(BF16)
+def slots_of(route_t, size, first):
+    rows = route_t.shape[1]
     expert = lax.broadcasted_iota(jnp.int32, (EXPERTS, rows), 0)
     named = jnp.zeros((EXPERTS, rows), F32)
-    weight = jnp.zeros((EXPERTS, rows), F32)
     for k in range(TOP):
-        hit = route_t[k : k + 1, :] == expert
-        named = named + jnp.where(hit, 1.0, 0.0)
-        weight = weight + jnp.where(hit, weight_t[k : k + 1, :], 0.0)
+        named = named + jnp.where(route_t[k : k + 1, :] == expert, 1.0, 0.0)
     earlier = lax.broadcasted_iota(jnp.int32, (rows, rows), 0) < lax.broadcasted_iota(
         jnp.int32, (rows, rows), 1
     )
@@ -47,14 +39,51 @@
         preferred_element_type=F32,
     )
     rank = jnp.where(named > 0.5, rank, -1.0)
-    slot = lax.broadcasted_iota(jnp.int32, (EXPERTS, CAP, rows), 1).astype(F32)
-    taken = rank[:, None, :] == slot
-    scatter = jnp.where(taken, 1.0, 0.0).reshape(EXPERTS * CAP, rows)
-    buffer[...] = jnp.dot(scatter.astype(BF16), normed, preferred_element_type=F32).astype(BF16)
+    slot = lax.broadcasted_iota(jnp.int32, (EXPERTS, size, rows), 1) + first
+    return rank[:, None, :] == slot.astype(F32)
+
+
+def prep_kernel(where, tokens, route_t, buffer):
+    rows, _ = tokens.shape
+    cols = buffer.shape[2]
+    floated = tokens[...].astype(F32)
+    inv = lax.rsqrt(jnp.mean(floated * floated, axis=-1, keepdims=True) + 1e-06)
+    for i, (size, first, at) in enumerate(((CAP, 0, 0), (CAP // 2, where[2], CAP))):
+        part = tokens[:, pl.ds(pl.multiple_of(where[i] * cols, cols), cols)].astype(F32)
+        normed = (part * inv).astype(BF16)
+        scatter = jnp.where(slots_of(route_t, size, first), 1.0, 0.0).reshape(EXPERTS * size, rows)
+        put = jnp.dot(scatter.astype(BF16), normed, preferred_element_type=F32)
+        buffer[:, at : at + size, :] = put.reshape(EXPERTS, size, cols).astype(BF16)
+
+
+def comb_kernel(route_t, weight_t, comb_hi, comb_lo):
+    rows = route_t.shape[1]
+    expert = lax.broadcasted_iota(jnp.int32, (EXPERTS, rows), 0)
+    weight = jnp.zeros((EXPERTS, rows), F32)
+    for k in range(TOP):
+        hit = route_t[k : k + 1, :] == expert
+        weight = weight + jnp.where(hit, weight_t[k : k + 1, :], 0.0)
+    taken = slots_of(route_t, CAP, 0)
     comb = jnp.where(taken, weight[:, None, :], 0.0).reshape(EXPERTS * CAP, rows)
     high = comb.astype(BF16)
     comb_hi[...] = high
     comb_lo[...] = (comb - high.astype(F32)).astype(BF16)
+
+
+def repack_kernel(got, own, low, high):
+    half = SUB // 2
+    for k in range(SUB - 1):
+        block = got[k, :, :CAP, :]
+        own[k] = block
+        if k < half:
+            low[k] = block
+        else:
+            high[k - half] = block
+    for j in range(2):
+        at = slice(j * CAP // 2, (j + 1) * CAP // 2)
+        block = got[1 + j, :, CAP:, :]
+        own[SUB - 1, :, at, :] = block
+        high[SUB - 1 - half, :, at, :] = block
 
 
 def pieces(own, first, second, low, high, res, stride):
@@ -158,17 +187,19 @@
     return lax.optimization_barrier((x, *others))[0]
 
 
-def gather(block):
+def strided(x):
     count = lax.axis_size("fs")
     stride = count // SUB
     groups = [[i + stride * j for j in range(SUB)] for i in range(stride)]
-    own = lax.all_gather(block, "fs", axis=0, axis_index_groups=groups)
+    return lax.all_gather(x, "fs", axis=0, axis_index_groups=groups)
+
+
+def neighbours(own, low, high):
+    count = lax.axis_size("fs")
 
     def swap(x, partner):
         return lax.ppermute(x, "fs", [(i, partner(i) % count) for i in range(count)])
 
-    half = SUB // 2
-    low, high = own[:half], own[half:]
     return [
         own,
         swap(own, lambda i: i ^ 1),
@@ -176,6 +207,13 @@
         swap(low, lambda i: i ^ 2),
         swap(high, lambda i: i + 2 if i & 2 else i - 2),
     ]
+
+
+def gather(block):
+    own = strided(block)
+    half = SUB // 2
+    low, high = own[:half], own[half:]
+    return neighbours(own, low, high)
 
 
 def other_groups(x):
@@ -202,18 +240,38 @@
     my_group = lax.axis_index("grp").astype(jnp.int32)
     ids = jnp.stack([my_block % stride, my_group])
 
-    buffer, comb_hi, comb_lo = pl.pallas_call(
-        prep_kernel,
-        in_specs=[sm(), vm(), vm(), vm()],
-        out_specs=[vm(), vm(), vm()],
-        out_shape=[
-            jax.ShapeDtypeStruct((slots, cols), BF16),
-            jax.ShapeDtypeStruct((slots, tok_rows), BF16),
-            jax.ShapeDtypeStruct((slots, tok_rows), BF16),
-        ],
-        name="prep",
-    )(my_block.reshape(1), tokens, route_expert.T, route_weight.T)
-    arrived = exchange(buffer.reshape(EXPERTS, CAP, cols)).reshape(slots, cols)
+    place = my_block // stride
+    where = jnp.stack(
+        [
+            my_block,
+            my_block % stride + fs_count - stride,
+            jnp.where(place == 2, CAP // 2, 0).astype(jnp.int32),
+        ]
+    )
+    route_t = route_expert.T
+    sent = jax.ShapeDtypeStruct((EXPERTS, CAP + CAP // 2, cols), BF16)
+
+    def send(where, tokens, route_t):
+        buffer = pl.pallas_call(
+            prep_kernel,
+            in_specs=[sm(), vm(), vm()],
+            out_specs=vm(),
+            out_shape=sent,
+            name="prep",
+        )(where, tokens, route_t)
+        return exchange(buffer)
+
+    def skip(where, tokens, route_t):
+        return jnp.zeros(sent.shape, sent.dtype)
+
+    arrived = lax.cond(place < SUB - 1, send, skip, where, tokens, route_t)
+    comb_hi, comb_lo = pl.pallas_call(
+        comb_kernel,
+        in_specs=[vm(), vm()],
+        out_specs=[vm(), vm()],
+        out_shape=[jax.ShapeDtypeStruct((slots, tok_rows), BF16)] * 2,
+        name="comb",
+    )(route_t, route_weight.T)
 
     size = gate_train.shape[1] // parts
 
@@ -228,6 +286,18 @@
     down_part = exchange(after(share(down_train).astype(BF16), both))
     served = jax.ShapeDtypeStruct(down_train.shape, BF16)
     hbm = pl.BlockSpec(memory_space=pl.ANY)
+
+    small = pltpu.CompilerParams(vmem_limit_bytes=16 << 20)
+    filled = [(k, EXPERTS, CAP, cols) for k in (SUB, SUB // 2, SUB // 2)]
+    packs = pl.pallas_call(
+        repack_kernel,
+        in_specs=[vm()],
+        out_specs=[vm()] * 3,
+        out_shape=[jax.ShapeDtypeStruct(shape, BF16) for shape in filled],
+        compiler_params=small,
+        name="repack",
+    )(*in_vmem([strided(arrived)]))
+    token_blocks = neighbours(*[p.reshape(p.shape[0], slots, cols) for p in packs])
 
     hidden, gate_serve, up_serve = pl.pallas_call(
         functools.partial(gate_up_kernel, stride=stride, parts=parts),
@@ -240,7 +310,7 @@
         ],
         compiler_params=pltpu.CompilerParams(vmem_limit_bytes=16 << 20),
         name="gate_up",
-    )(ids, *in_vmem(gather(arrived) + other_groups(both)))
+    )(ids, *in_vmem(token_blocks + other_groups(both)))
     expert_out, down_serve = pl.pallas_call(
         functools.partial(down_kernel, stride=stride, parts=parts),
         in_specs=[sm()] + [vm()] * (5 + parts),

time: 296 us -> 297 us (level)
  waiting for transfers between devices: 62.9 us -> 68.9 us
  starting transfers between devices: 73.5 us -> 69.2 us
  blocking collectives: 144 us -> 140 us
    ppermute x8, starting transfers between devices: 43.1 us -> 33.8 us  [swap(): lax.ppermute(x, 'fs', [(i, partner(i) % count) for i in range(count)])]
    ppermute x2, starting transfers between devices: 5.62 us -> 13.2 us  [other_groups(): lax.ppermute(x, 'grp', [(i, (i + k) % count) for i in range(count)])]
    ppermute x8, waiting for transfers between devices: 16.2 us -> 21.5 us  [swap(): lax.ppermute(x, 'fs', [(i, partner(i) % count) for i in range(count)])]
    all_gather x2, blocking collectives: 110 us -> 106 us  [strided(): return lax.all_gather(x, 'fs', axis=0, axis_index_groups=groups)]
  transfers between devices with their start and end apart: 13 -> 13, of which waited for: 5 -> 6; matrix products, arithmetic and copies ran while one was open for 1% -> 1% of each run, Pallas kernels for 2% -> 1%
where the time goes in v4:
time: 297 us; the launch traced here: 295 us
  blocking collectives  140 us (47%)
  starting transfers between devices  69.2 us (23%)
  waiting for transfers between devices  68.9 us (23%)
  Pallas kernels  8.71 us (3%)
  local copies, waits for them, and re-layouts  4.84 us (2%)
    all_gather x2, blocking collectives, strided(): return lax.all_gather(x, 'fs', axis=0, axis_index_groups=groups)  106 us
    all_to_all x3, waiting for transfers between devices, exchange(): return lax.all_to_all(x, 'tp', split_axis=0, concat_axis=0, tiled=True)  47.3 us
    all_to_all x1, blocking collectives, exchange(): return lax.all_to_all(x, 'tp', split_axis=0, concat_axis=0, tiled=True)  34.5 us
    ppermute x8, starting transfers between devices, swap(): lax.ppermute(x, 'fs', [(i, partner(i) % count) for i in range(count)])  33.8 us
    all_to_all x3, starting transfers between devices, exchange(): return lax.all_to_all(x, 'tp', split_axis=0, concat_axis=0, tiled=True)  22.2 us
    ppermute x8, waiting for transfers between devices, swap(): lax.ppermute(x, 'fs', [(i, partner(i) % count) for i in range(count)])  21.5 us
    ppermute x2, starting transfers between devices, other_groups(): lax.ppermute(x, 'grp', [(i, (i + k) % count) for i in range(count)])  13.2 us
  transfers between devices with their start and end apart: 13, of which 6 were waited for; matrix products, arithmetic and copies ran while one was open for 1% of the time, Pallas kernels for 1%

profile of v4, /device:TPU:6, one launch (start us, length us, event | category | flops | bytes accessed | tf_op | source)
XLA Modules:
  0.0 295.1 jit_solution(5226441443274934944)
XLA Ops:
  1.5 1.4 multiply_convert_fusion.1
  2.9 0.9 pad_maximum_fusion
  4.5 36.1 %conditional.1 = (bf16[32,24,128]{2,1,0:T(8,128)(2,1)S(1)}) conditional(s32[]{:T(128)} %convert_element_type.12, () %tuple.16, (s32[3]{0:T(128)S(1)}, bf16[120,2048]{1,0:T(8,128)(2,1)S(1)}, s32[4,120]{1,0:T(4,128)S(1)}) %tuple.26), branch_computations={%region_0.1_spmd, %region_1.2_spmd} | conditional | bytes 393224 | solution.py:267
  4.5 1.6 prep.1
  6.1 34.5 %all_to_all.19 = bf16[32,24,128]{2,1,0:T(8,128)(2,1)S(1)} all-to-all(bf16[32,24,128]{2,1,0:T(8,128)(2,1)} %prep.1), channel_id=1, replica_groups=mesh['grp'=2,'fs'=16,'tp'=32] {'tp'}, dimensions={0} | all-to-all | bytes 393216 | tf_op jit(solution)/shard_map/cond/branch_1_fun/all_to_all | solution.py:183
  40.5 4.8 %all-to-all-start.1 = ((bf16[32,64,128]{2,1,0:T(8,128)(2,1)}), bf16[32,64,128]{2,1,0:T(8,128)(2,1)S(1)}, u32[]{:S(2)}, u32[]{:S(2)}) async-start(bf16[32,64,128]{2,1,0:T(8,128)(2,1)} %pad_maximum_fusion), calls=%async_computation.1 | async-start | bytes 1048576 | tf_op jit(solution)/shard_map/all_to_all | solution.py:183
  46.1 32.4 %all-to-all-done.1.refs_5_ = bf16[32,64,128]{2,1,0:T(8,128)(2,1)S(1)} async-done(((bf16[32,64,128]{2,1,0:T(8,128)(2,1)}), bf16[32,64,128]{2,1,0:T(8,128)(2,1)S(1)}, u32[]{:S(2)}, u32[]{:S(2)}) %all-to-all-start.1) | async-done | bytes 524320 | tf_op jit(solution)/shard_map/all_to_all | solution.py:183
  78.5 4.8 %all-to-all-start.2 = ((bf16[32,32,128]{2,1,0:T(8,128)(2,1)}), bf16[32,32,128]{2,1,0:T(8,128)(2,1)S(1)}, u32[]{:S(2)}, u32[]{:S(2)}) async-start(bf16[32,32,128]{2,1,0:T(8,128)(2,1)} %dynamic-slice_convert_fusion), calls=%async_computation.2 | async-start | bytes 524288 | tf_op jit(solution)/shard_map/all_to_all | solution.py:183
  83.3 78.5 %all-gather = bf16[128,24,128]{2,1,0:T(8,128)(2,1)S(1)} all-gather(bf16[32,24,128]{2,1,0:T(8,128)(2,1)S(1)} %get-tuple-element.46), channel_id=2, replica_groups={{0,128,256,384},{32,160,288,416},{64,192,320,448},{96,224,352,480},{1,1..., dimensions={0}, use_global_device_ids=true | all-gather | bytes 983040 | tf_op jit(solution)/shard_map/all_gather | solution.py:194
  162.0 7.3 %collective-permute-start = (bf16[4,512,128]{2,1,0:T(8,128)(2,1)S(1)}, bf16[4,512,128]{2,1,0:T(8,128)(2,1)S(1)}, u32[]{:S(2)}, u32[]{:S(2)}) collective-permute-start(bf16[4,512,128]{2,1,0:T(8,128)(2,1)S(1)} %bitcast.24), channel_id=1, source_target_pairs={{0,32},{32,0},{64,96},{96,64},{128,160},{160,128},{192,224},{224,1... | collective-permute-start | bytes 1572872 | tf_op jit(solution)/shard_map/ppermute | solution.py:201
  169.3 7.9 %collective-permute-start.1 = (bf16[4,512,128]{2,1,0:T(8,128)(2,1)S(1)}, bf16[4,512,128]{2,1,0:T(8,128)(2,1)S(1)}, u32[]{:S(2)}, u32[]{:S(2)}) collective-permute-start(bf16[4,512,128]{2,1,0:T(8,128)(2,1)S(1)} %bitcast.25), channel_id=1, source_target_pairs={{0,480},{32,64},{64,32},{96,128},{128,96},{160,192},{192,160},{224... | collective-permute-start | bytes 1572872 | tf_op jit(solution)/shard_map/ppermute | solution.py:201
  177.2 9.5 %collective-permute-start.4 = (bf16[32,64,128]{2,1,0:T(8,128)(2,1)S(1)}, bf16[32,64,128]{2,1,0:T(8,128)(2,1)S(1)}, u32[]{:S(2)}, u32[]{:S(2)}) collective-permute-start(bf16[32,64,128]{2,1,0:T(8,128)(2,1)S(1)} %all-to-all-done.1.refs_5_), channel_id=1, source_target_pairs={{0,512},{512,0},{1,513},{513,1},{2,514},{514,2},{3,515},{515,3},{4... | collective-permute-start | bytes 1572872 | tf_op jit(solution)/shard_map/ppermute | solution.py:222
  186.8 5.4 %collective-permute-start.2 = (bf16[2,512,128]{2,1,0:T(8,128)(2,1)S(1)}, bf16[2,512,128]{2,1,0:T(8,128)(2,1)S(1)}, u32[]{:S(2)}, u32[]{:S(2)}) collective-permute-start(bf16[2,512,128]{2,1,0:T(8,128)(2,1)S(1)} %bitcast.28), channel_id=1, source_target_pairs={{0,64},{32,96},{64,0},{96,32},{128,192},{160,224},{192,128},{224,1... | collective-permute-start | bytes 786440 | tf_op jit(solution)/shard_map/ppermute | solution.py:201
  192.2 2.0 collective-permute-start.3
  194.2 8.0 %collective-permute-done.2.refs_3_ = bf16[2,512,128]{2,1,0:T(8,128)(2,1)S(1)} collective-permute-done((bf16[2,512,128]{2,1,0:T(8,128)(2,1)S(1)}, bf16[2,512,128]{2,1,0:T(8,128)(2,1)S(1)}, u32[]{:S(2)}, u32[]{:S(2)}) %collective-permute-start.2) | collective-permute-done | bytes 262176 | tf_op jit(solution)/shard_map/ppermute | solution.py:201
  202.3 5.4 %collective-permute-done.3.refs_4_ = bf16[2,512,128]{2,1,0:T(8,128)(2,1)S(1)} collective-permute-done((bf16[2,512,128]{2,1,0:T(8,128)(2,1)S(1)}, bf16[2,512,128]{2,1,0:T(8,128)(2,1)S(1)}, u32[]{:S(2)}, u32[]{:S(2)}) %collective-permute-start.3) | collective-permute-done | bytes 262176 | tf_op jit(solution)/shard_map/ppermute | solution.py:201
  207.7 2.1 gate_up.1
  209.8 27.2 %all-gather.1 = bf16[2048,128]{1,0:T(8,128)(2,1)S(1)} all-gather(bf16[512,128]{1,0:T(8,128)(2,1)S(1)} %get-tuple-element.34), channel_id=3, replica_groups={{0,128,256,384},{32,160,288,416},{64,192,320,448},{96,224,352,480},{1,1..., dimensions={0}, use_global_device_ids=true | all-gather | bytes 655360 | tf_op jit(solution)/shard_map/all_gather | solution.py:194
  237.0 1.9 collective-permute-start.5
  239.0 2.0 collective-permute-start.6
  241.8 5.4 %collective-permute-start.7 = (bf16[2,512,128]{2,1,0:T(8,128)(2,1)}, bf16[2,512,128]{2,1,0:T(8,128)(2,1)S(1)}, u32[]{:S(2)}, u32[]{:S(2)}) collective-permute-start(bf16[2,512,128]{2,1,0:T(8,128)(2,1)} %bitcast.13), channel_id=1, source_target_pairs={{0,64},{32,96},{64,0},{96,32},{128,192},{160,224},{192,128},{224,1... | collective-permute-start | bytes 786440 | tf_op jit(solution)/shard_map/ppermute | solution.py:201
  247.2 2.0 collective-permute-start.8
  249.1 3.6 %collective-permute-start.9 = (bf16[32,32,128]{2,1,0:T(8,128)(2,1)S(1)}, bf16[32,32,128]{2,1,0:T(8,128)(2,1)S(1)}, u32[]{:S(2)}, u32[]{:S(2)}) collective-permute-start(bf16[32,32,128]{2,1,0:T(8,128)(2,1)S(1)} %all-to-all-done.2.refs_5_), channel_id=1, source_target_pairs={{0,512},{512,0},{1,513},{513,1},{2,514},{514,2},{3,515},{515,3},{4... | collective-permute-start | bytes 786440 | tf_op jit(solution)/shard_map/ppermute | solution.py:222
  252.7 6.3 %collective-permute-done.7.refs_3_ = bf16[2,512,128]{2,1,0:T(8,128)(2,1)S(1)} collective-permute-done((bf16[2,512,128]{2,1,0:T(8,128)(2,1)}, bf16[2,512,128]{2,1,0:T(8,128)(2,1)S(1)}, u32[]{:S(2)}, u32[]{:S(2)}) %collective-permute-start.7) | collective-permute-done | bytes 262176 | tf_op jit(solution)/shard_map/ppermute | solution.py:201
  259.0 1.8 collective-permute-done.8.refs_4_
  260.8 2.4 down.1
  263.3 12.6 %all-to-all-start.3 = ((bf16[32,16,128]{2,1,0:T(8,128)(2,1)}), bf16[32,16,128]{2,1,0:T(8,128)(2,1)S(1)}, u32[]{:S(2)}, u32[]{:S(2)}) async-start(bf16[32,16,128]{2,1,0:T(8,128)(2,1)} %bitcast.17), calls=%async_computation.3 | async-start | bytes 262144 | tf_op jit(solution)/shard_map/all_to_all | solution.py:183
  275.9 1.6 comb.1
  277.5 14.9 %all-to-all-done.3 = bf16[32,16,128]{2,1,0:T(8,128)(2,1)S(1)} async-done(((bf16[32,16,128]{2,1,0:T(8,128)(2,1)}), bf16[32,16,128]{2,1,0:T(8,128)(2,1)S(1)}, u32[]{:S(2)}, u32[]{:S(2)}) %all-to-all-start.3) | async-done | bytes 131104 | tf_op jit(solution)/shard_map/all_to_all | solution.py:183
  292.4 0.9 copy-done.1
  293.3 0.9 copy-done.2
  294.2 0.9 combine.1
  (23 shorter events, 3.3 us)
Async XLA Ops:
  0.6 44.7 %copy-start = (f32[32,64,128]{2,1,0:T(8,128)S(1)}, f32[32,64,128]{2,1,0:T(8,128)}, u32[]{:S(2)}) copy-start(f32[32,64,128]{2,1,0:T(8,128)} %param.15) | copy-start | bytes 3145732
  0.7 0.7 copy-start.5
  2.9 1.2 copy-start.3
  3.7 0.7 copy-start.4
  40.5 38.0 %all-to-all-start.1 = ((bf16[32,64,128]{2,1,0:T(8,128)(2,1)}), bf16[32,64,128]{2,1,0:T(8,128)(2,1)S(1)}, u32[]{:S(2)}, u32[]{:S(2)}) async-start(bf16[32,64,128]{2,1,0:T(8,128)(2,1)} %pad_maximum_fusion), calls=%async_computation.1 | async-start | bytes 1048576 | tf_op jit(solution)/shard_map/all_to_all | solution.py:183
  78.5 170.6 %all-to-all-start.2 = ((bf16[32,32,128]{2,1,0:T(8,128)(2,1)}), bf16[32,32,128]{2,1,0:T(8,128)(2,1)S(1)}, u32[]{:S(2)}, u32[]{:S(2)}) async-start(bf16[32,32,128]{2,1,0:T(8,128)(2,1)} %dynamic-slice_convert_fusion), calls=%async_computation.2 | async-start | bytes 524288 | tf_op jit(solution)/shard_map/all_to_all | solution.py:183
  162.0 45.7 %collective-permute-start = (bf16[4,512,128]{2,1,0:T(8,128)(2,1)S(1)}, bf16[4,512,128]{2,1,0:T(8,128)(2,1)S(1)}, u32[]{:S(2)}, u32[]{:S(2)}) collective-permute-start(bf16[4,512,128]{2,1,0:T(8,128)(2,1)S(1)} %bitcast.24), channel_id=1, source_target_pairs={{0,32},{32,0},{64,96},{96,64},{128,160},{160,128},{192,224},{224,1... | collective-permute-start | bytes 1572872 | tf_op jit(solution)/shard_map/ppermute | solution.py:201
  169.3 38.4 %collective-permute-start.1 = (bf16[4,512,128]{2,1,0:T(8,128)(2,1)S(1)}, bf16[4,512,128]{2,1,0:T(8,128)(2,1)S(1)}, u32[]{:S(2)}, u32[]{:S(2)}) collective-permute-start(bf16[4,512,128]{2,1,0:T(8,128)(2,1)S(1)} %bitcast.25), channel_id=1, source_target_pairs={{0,480},{32,64},{64,32},{96,128},{128,96},{160,192},{192,160},{224... | collective-permute-start | bytes 1572872 | tf_op jit(solution)/shard_map/ppermute | solution.py:201
  177.2 30.5 %collective-permute-start.4 = (bf16[32,64,128]{2,1,0:T(8,128)(2,1)S(1)}, bf16[32,64,128]{2,1,0:T(8,128)(2,1)S(1)}, u32[]{:S(2)}, u32[]{:S(2)}) collective-permute-start(bf16[32,64,128]{2,1,0:T(8,128)(2,1)S(1)} %all-to-all-done.1.refs_5_), channel_id=1, source_target_pairs={{0,512},{512,0},{1,513},{513,1},{2,514},{514,2},{3,515},{515,3},{4... | collective-permute-start | bytes 1572872 | tf_op jit(solution)/shard_map/ppermute | solution.py:222
  186.8 15.5 %collective-permute-start.2 = (bf16[2,512,128]{2,1,0:T(8,128)(2,1)S(1)}, bf16[2,512,128]{2,1,0:T(8,128)(2,1)S(1)}, u32[]{:S(2)}, u32[]{:S(2)}) collective-permute-start(bf16[2,512,128]{2,1,0:T(8,128)(2,1)S(1)} %bitcast.28), channel_id=1, source_target_pairs={{0,64},{32,96},{64,0},{96,32},{128,192},{160,224},{192,128},{224,1... | collective-permute-start | bytes 786440 | tf_op jit(solution)/shard_map/ppermute | solution.py:201
  192.2 15.5 %collective-permute-start.3 = (bf16[2,512,128]{2,1,0:T(8,128)(2,1)S(1)}, bf16[2,512,128]{2,1,0:T(8,128)(2,1)S(1)}, u32[]{:S(2)}, u32[]{:S(2)}) collective-permute-start(bf16[2,512,128]{2,1,0:T(8,128)(2,1)S(1)} %bitcast.27), channel_id=1, source_target_pairs={{0,448},{32,480},{64,128},{96,160},{128,64},{160,96},{192,256},{22... | collective-permute-start | bytes 786440 | tf_op jit(solution)/shard_map/ppermute | solution.py:201
  237.0 23.8 %collective-permute-start.5 = (bf16[4,512,128]{2,1,0:T(8,128)(2,1)S(1)}, bf16[4,512,128]{2,1,0:T(8,128)(2,1)S(1)}, u32[]{:S(2)}, u32[]{:S(2)}) collective-permute-start(bf16[4,512,128]{2,1,0:T(8,128)(2,1)S(1)} %bitcast.19), channel_id=1, source_target_pairs={{0,32},{32,0},{64,96},{96,64},{128,160},{160,128},{192,224},{224,1... | collective-permute-start | bytes 1572872 | tf_op jit(solution)/shard_map/ppermute | solution.py:201
  239.0 21.9 %collective-permute-start.6 = (bf16[4,512,128]{2,1,0:T(8,128)(2,1)S(1)}, bf16[4,512,128]{2,1,0:T(8,128)(2,1)S(1)}, u32[]{:S(2)}, u32[]{:S(2)}) collective-permute-start(bf16[4,512,128]{2,1,0:T(8,128)(2,1)S(1)} %bitcast.20), channel_id=1, source_target_pairs={{0,480},{32,64},{64,32},{96,128},{128,96},{160,192},{192,160},{224... | collective-permute-start | bytes 1572872 | tf_op jit(solution)/shard_map/ppermute | solution.py:201
  241.8 17.3 %collective-permute-start.7 = (bf16[2,512,128]{2,1,0:T(8,128)(2,1)}, bf16[2,512,128]{2,1,0:T(8,128)(2,1)S(1)}, u32[]{:S(2)}, u32[]{:S(2)}) collective-permute-start(bf16[2,512,128]{2,1,0:T(8,128)(2,1)} %bitcast.13), channel_id=1, source_target_pairs={{0,64},{32,96},{64,0},{96,32},{128,192},{160,224},{192,128},{224,1... | collective-permute-start | bytes 786440 | tf_op jit(solution)/shard_map/ppermute | solution.py:201
  247.2 13.7 %collective-permute-start.8 = (bf16[2,512,128]{2,1,0:T(8,128)(2,1)}, bf16[2,512,128]{2,1,0:T(8,128)(2,1)S(1)}, u32[]{:S(2)}, u32[]{:S(2)}) collective-permute-start(bf16[2,512,128]{2,1,0:T(8,128)(2,1)} %bitcast.14), channel_id=1, source_target_pairs={{0,448},{32,480},{64,128},{96,160},{128,64},{160,96},{192,256},{22... | collective-permute-start | bytes 786440 | tf_op jit(solution)/shard_map/ppermute | solution.py:201
  249.1 11.7 %collective-permute-start.9 = (bf16[32,32,128]{2,1,0:T(8,128)(2,1)S(1)}, bf16[32,32,128]{2,1,0:T(8,128)(2,1)S(1)}, u32[]{:S(2)}, u32[]{:S(2)}) collective-permute-start(bf16[32,32,128]{2,1,0:T(8,128)(2,1)S(1)} %all-to-all-done.2.refs_5_), channel_id=1, source_target_pairs={{0,512},{512,0},{1,513},{513,1},{2,514},{514,2},{3,515},{515,3},{4... | collective-permute-start | bytes 786440 | tf_op jit(solution)/shard_map/ppermute | solution.py:222
  263.3 29.1 %all-to-all-start.3 = ((bf16[32,16,128]{2,1,0:T(8,128)(2,1)}), bf16[32,16,128]{2,1,0:T(8,128)(2,1)S(1)}, u32[]{:S(2)}, u32[]{:S(2)}) async-start(bf16[32,16,128]{2,1,0:T(8,128)(2,1)} %bitcast.17), calls=%async_computation.3 | async-start | bytes 262144 | tf_op jit(solution)/shard_map/all_to_all | solution.py:183
  292.4 0.9 copy-start.1
  293.3 0.9 copy-start.2

commit v5 on v4

--- a/solution.py
+++ b/solution.py
@@ -99,6 +99,13 @@
     return out
 
 
+def pack_kernel(group, gate, up, down, gain, out):
+    size = gain.shape[0]
+    out[:, :size, :] = (gate[...] * gain[...]).astype(BF16)
+    out[:, size : 2 * size, :] = (up[...] * gain[...]).astype(BF16)
+    out[:, 2 * size :, :] = down[...].astype(BF16)
+
+
 def part_at(first, k, parts, size):
     return pl.ds(pl.multiple_of(((first + parts - k) % parts) * size, size), size)
 
@@ -107,7 +114,7 @@
     five, weights = refs[:5], refs[5 : 5 + parts]
     hidden, gate_out, up_out, whole, sems = refs[5 + parts :]
     rows, width = hidden.shape
-    size = weights[0].shape[1] // 2
+    size = weights[0].shape[1] // 3
     copies = []
     for k, w in enumerate(weights):
         at = part_at(ids[1], k, parts, size)
@@ -151,12 +158,13 @@
     five, weights = refs[:5], refs[5 : 5 + parts]
     out, down_out, whole, sems = refs[5 + parts :]
     rows, _ = out.shape
-    size = weights[0].shape[1]
+    size = weights[0].shape[1] // 3
     copies = []
     for k, w in enumerate(weights):
         at = part_at(ids[1], k, parts, size)
-        copies.append(pltpu.make_async_copy(w, down_out.at[:, at, :], sems.at[k]))
-        whole[:, at, :] = w[...]
+        src = w.at[:, 2 * size :, :]
+        copies.append(pltpu.make_async_copy(src, down_out.at[:, at, :], sems.at[k]))
+        whole[:, at, :] = w[:, 2 * size :, :]
     for c in copies:
         c.start()
     order = pieces(*five, ids[0], stride)
@@ -275,15 +283,22 @@
 
     size = gate_train.shape[1] // parts
 
-    def share(w):
-        return lax.dynamic_slice_in_dim(w, my_group * size, size, 1)
-
-    gain = lax.dynamic_slice_in_dim(norm_gain, my_group * size, size)[None, :, None]
-    packed = jnp.concatenate(
-        [(share(gate_train) * gain).astype(BF16), (share(up_train) * gain).astype(BF16)], axis=1
-    )
-    both = exchange(after(packed, arrived))
-    down_part = exchange(after(share(down_train).astype(BF16), both))
+    step = 8
+    taken = (step, size, gate_train.shape[2])
+    train_spec = pl.BlockSpec(taken, lambda i, group: (i, group[0], 0))
+    gain = jnp.broadcast_to(norm_gain[:, None], (norm_gain.shape[0], taken[2]))
+    packed = pl.pallas_call(
+        pack_kernel,
+        grid_spec=pltpu.PrefetchScalarGridSpec(
+            num_scalar_prefetch=1,
+            grid=(EXPERTS // step,),
+            in_specs=[train_spec] * 3 + [pl.BlockSpec(taken[1:], lambda i, group: (group[0], 0))],
+            out_specs=pl.BlockSpec((step, 3 * size, taken[2]), lambda i, group: (i, 0, 0)),
+        ),
+        out_shape=jax.ShapeDtypeStruct((EXPERTS, 3 * size, taken[2]), BF16),
+        name="pack",
+    )(my_group.reshape(1), gate_train, up_train, down_train, gain)
+    weights = in_vmem(other_groups(exchange(after(packed, arrived))))
     served = jax.ShapeDtypeStruct(down_train.shape, BF16)
     hbm = pl.BlockSpec(memory_space=pl.ANY)
 
@@ -303,14 +318,14 @@
         functools.partial(gate_up_kernel, stride=stride, parts=parts),
         in_specs=[sm()] + [vm()] * (5 + parts),
         out_specs=[vm(), hbm, hbm],
-        out_shape=[jax.ShapeDtypeStruct((slots, both.shape[2]), BF16), served, served],
+        out_shape=[jax.ShapeDtypeStruct((slots, gate_train.shape[2]), BF16), served, served],
         scratch_shapes=[
-            pltpu.VMEM(served.shape[:2] + (2 * both.shape[2],), BF16),
+            pltpu.VMEM(served.shape[:2] + (2 * gate_train.shape[2],), BF16),
             pltpu.SemaphoreType.DMA((2 * parts,)),
         ],
         compiler_params=pltpu.CompilerParams(vmem_limit_bytes=16 << 20),
         name="gate_up",
-    )(ids, *in_vmem(token_blocks + other_groups(both)))
+    )(ids, *in_vmem(token_blocks), *weights)
     expert_out, down_serve = pl.pallas_call(
         functools.partial(down_kernel, stride=stride, parts=parts),
         in_specs=[sm()] + [vm()] * (5 + parts),
@@ -322,7 +337,7 @@
         ],
         compiler_params=pltpu.CompilerParams(vmem_limit_bytes=16 << 20),
         name="down",
-    )(ids, *in_vmem(gather(hidden) + other_groups(down_part)))
+    )(ids, *in_vmem(gather(hidden)), *weights)
     returned = exchange(expert_out.reshape(tp_count, slots // tp_count, -1)).reshape(slots, -1)
     mixed = pl.pallas_call(
         combine_kernel,

time: 297 us -> 300 us (1.010)
  starting transfers between devices: 69.2 us -> 104 us
  waiting for transfers between devices: 68.9 us -> 43.7 us
  blocking collectives: 140 us -> 132 us
  Pallas kernels: 8.71 us -> 12.7 us
    ppermute x2 -> x1, starting transfers between devices: 13.2 us -> 73.9 us  [other_groups(): lax.ppermute(x, 'grp', [(i, (i + k) % count) for i in range(count)])]
    all_gather x2, blocking collectives: 106 us -> 48.8 us  [strided(): return lax.all_gather(x, 'fs', axis=0, axis_index_groups=groups)]
    all_to_all x1 -> x2, blocking collectives: 34.5 us -> 83.7 us  [exchange(): return lax.all_to_all(x, 'tp', split_axis=0, concat_axis=0, tiled=True)]
    all_to_all x3 -> x1, waiting for transfers between devices: 47.3 us -> 14.8 us  [exchange(): return lax.all_to_all(x, 'tp', split_axis=0, concat_axis=0, tiled=True)]
    all_to_all x3 -> x1, starting transfers between devices: 22.2 us -> 4.77 us  [exchange(): return lax.all_to_all(x, 'tp', split_axis=0, concat_axis=0, tiled=True)]
    ppermute x8, starting transfers between devices: 33.8 us -> 25.1 us  [swap(): lax.ppermute(x, 'fs', [(i, partner(i) % count) for i in range(count)])]
    ppermute x8, waiting for transfers between devices: 21.5 us -> 28.9 us  [swap(): lax.ppermute(x, 'fs', [(i, partner(i) % count) for i in range(count)])]
    pallas_call x0 -> x1, Pallas kernels: none -> 3.46 us  [body(): pl.pallas_call(pack_kernel, grid_spec=pltpu.PrefetchScalarGridSpec(num_sc...]
  transfers between devices with their start and end apart: 13 -> 10, of which waited for: 6 -> 3; matrix products, arithmetic and copies ran while one was open for 1% -> 0% of each run, Pallas kernels for 1% -> 1%
where the time goes in v5:
time: 300 us; the launch traced here: 297 us
  blocking collectives  132 us (44%)
  starting transfers between devices  104 us (35%)
  waiting for transfers between devices  43.7 us (15%)
  Pallas kernels  12.7 us (4%)
  local copies, waits for them, and re-layouts  3.79 us (1%)
    all_to_all x2, blocking collectives, exchange(): return lax.all_to_all(x, 'tp', split_axis=0, concat_axis=0, tiled=True)  83.7 us
    ppermute x1, starting transfers between devices, other_groups(): lax.ppermute(x, 'grp', [(i, (i + k) % count) for i in range(count)])  73.9 us
    all_gather x2, blocking collectives, strided(): return lax.all_gather(x, 'fs', axis=0, axis_index_groups=groups)  48.8 us
    ppermute x8, waiting for transfers between devices, swap(): lax.ppermute(x, 'fs', [(i, partner(i) % count) for i in range(count)])  28.9 us
    ppermute x8, starting transfers between devices, swap(): lax.ppermute(x, 'fs', [(i, partner(i) % count) for i in range(count)])  25.1 us
    all_to_all x1, waiting for transfers between devices, exchange(): return lax.all_to_all(x, 'tp', split_axis=0, concat_axis=0, tiled=True)  14.8 us
  transfers between devices with their start and end apart: 10, of which 3 were waited for; matrix products, arithmetic and copies ran while one was open for 0% of the time, Pallas kernels for 1%

profile of v5, /device:TPU:6, one launch (start us, length us, event | category | flops | bytes accessed | tf_op | source)
XLA Modules:
  0.0 297.3 jit_solution(3780868489975145767)
XLA Ops:
  0.7 0.1 pad_add_fusion.1
  0.7 0.6 copy-done.2
  1.3 36.6 %conditional.1 = (bf16[32,24,128]{2,1,0:T(8,128)(2,1)S(1)}) conditional(s32[]{:T(128)} %convert_element_type.3, () %tuple.15, (s32[3]{0:T(128)S(1)}, bf16[120,2048]{1,0:T(8,128)(2,1)}, s32[4,120]{1,0:T(4,128)S(1)}) %tuple.22), branch_computations={%region_0.1_spmd, %region_1.2_spmd} | conditional | bytes 393224 | solution.py:275
  1.3 2.1 prep.1
  3.5 34.5 %all_to_all.14 = bf16[32,24,128]{2,1,0:T(8,128)(2,1)S(1)} all-to-all(bf16[32,24,128]{2,1,0:T(8,128)(2,1)} %prep.1), channel_id=1, replica_groups=mesh['grp'=2,'fs'=16,'tp'=32] {'tp'}, dimensions={0} | all-to-all | bytes 393216 | tf_op jit(solution)/shard_map/cond/branch_1_fun/all_to_all | solution.py:191
  37.9 0.7 copy-done.3
  38.6 0.7 broadcast_in_dim.2.gain
  39.3 3.5 %pack.1 = bf16[32,96,128]{2,1,0:T(8,128)(2,1)} custom-call(s32[1]{0:T(128)} %bitcast.1.group, f32[32,64,128]{2,1,0:T(8,128)} %gate.1, f32[32,64,128]{2,1,0:T(8,128)} %up.1, f32[32,64,128]{2,1,0:T(8,128)} %down.2, f32[64,128]{1,0:T(8,128)} %broadcast_in_dim.2.gain), custom_call_target="tpu_custom_call" | custom-call | tf_op jit(solution)/shard_map/pack/pallas_call | solution.py:290
  42.7 49.2 %all_to_all.15.refs_5_ = bf16[32,96,128]{2,1,0:T(8,128)(2,1)S(1)} all-to-all(bf16[32,96,128]{2,1,0:T(8,128)(2,1)} %pack.1), channel_id=1, replica_groups=mesh['grp'=2,'fs'=16,'tp'=32] {'tp'}, dimensions={0} | all-to-all | bytes 1572864 | tf_op jit(solution)/shard_map/all_to_all | solution.py:191
  92.0 73.9 %collective-permute-start.4 = (bf16[32,96,128]{2,1,0:T(8,128)(2,1)S(1)}, bf16[32,96,128]{2,1,0:T(8,128)(2,1)S(1)}, u32[]{:S(2)}, u32[]{:S(2)}) collective-permute-start(bf16[32,96,128]{2,1,0:T(8,128)(2,1)S(1)} %all_to_all.15.refs_5_), channel_id=1, source_target_pairs={{0,512},{512,0},{1,513},{513,1},{2,514},{514,2},{3,515},{515,3},{4... | collective-permute-start | bytes 2359304 | tf_op jit(solution)/shard_map/ppermute | solution.py:230
  165.8 25.4 %all-gather = bf16[128,24,128]{2,1,0:T(8,128)(2,1)S(1)} all-gather(bf16[32,24,128]{2,1,0:T(8,128)(2,1)S(1)} %get-tuple-element.42), channel_id=2, replica_groups={{0,128,256,384},{32,160,288,416},{64,192,320,448},{96,224,352,480},{1,1..., dimensions={0}, use_global_device_ids=true | all-gather | bytes 983040 | tf_op jit(solution)/shard_map/all_gather | solution.py:202
  191.3 0.1 repack.1
  191.4 2.0 collective-permute-start
  193.4 2.0 collective-permute-start.1
  195.3 5.4 %collective-permute-start.2 = (bf16[2,512,128]{2,1,0:T(8,128)(2,1)S(1)}, bf16[2,512,128]{2,1,0:T(8,128)(2,1)S(1)}, u32[]{:S(2)}, u32[]{:S(2)}) collective-permute-start(bf16[2,512,128]{2,1,0:T(8,128)(2,1)S(1)} %bitcast.28), channel_id=1, source_target_pairs={{0,64},{32,96},{64,0},{96,32},{128,192},{160,224},{192,128},{224,1... | collective-permute-start | bytes 786440 | tf_op jit(solution)/shard_map/ppermute | solution.py:209
  200.7 2.0 collective-permute-start.3
  202.7 0.1 pad_add_fusion.ids
  202.8 16.4 %collective-permute-done.2.refs_3_ = bf16[2,512,128]{2,1,0:T(8,128)(2,1)S(1)} collective-permute-done((bf16[2,512,128]{2,1,0:T(8,128)(2,1)S(1)}, bf16[2,512,128]{2,1,0:T(8,128)(2,1)S(1)}, u32[]{:S(2)}, u32[]{:S(2)}) %collective-permute-start.2) | collective-permute-done | bytes 262176 | tf_op jit(solution)/shard_map/ppermute | solution.py:209
  219.2 2.1 gate_up.1
  221.3 23.4 %all-gather.1 = bf16[2048,128]{1,0:T(8,128)(2,1)S(1)} all-gather(bf16[512,128]{1,0:T(8,128)(2,1)S(1)} %get-tuple-element.33), channel_id=3, replica_groups={{0,128,256,384},{32,160,288,416},{64,192,320,448},{96,224,352,480},{1,1..., dimensions={0}, use_global_device_ids=true | all-gather | bytes 655360 | tf_op jit(solution)/shard_map/all_gather | solution.py:202
  244.7 3.7 %collective-permute-start.5 = (bf16[4,512,128]{2,1,0:T(8,128)(2,1)S(1)}, bf16[4,512,128]{2,1,0:T(8,128)(2,1)S(1)}, u32[]{:S(2)}, u32[]{:S(2)}) collective-permute-start(bf16[4,512,128]{2,1,0:T(8,128)(2,1)S(1)} %bitcast.19), channel_id=1, source_target_pairs={{0,32},{32,0},{64,96},{96,64},{128,160},{160,128},{192,224},{224,1... | collective-permute-start | bytes 1572872 | tf_op jit(solution)/shard_map/ppermute | solution.py:209
  248.4 4.1 %collective-permute-start.6 = (bf16[4,512,128]{2,1,0:T(8,128)(2,1)S(1)}, bf16[4,512,128]{2,1,0:T(8,128)(2,1)S(1)}, u32[]{:S(2)}, u32[]{:S(2)}) collective-permute-start(bf16[4,512,128]{2,1,0:T(8,128)(2,1)S(1)} %bitcast.20), channel_id=1, source_target_pairs={{0,480},{32,64},{64,32},{96,128},{128,96},{160,192},{192,160},{224... | collective-permute-start | bytes 1572872 | tf_op jit(solution)/shard_map/ppermute | solution.py:209
  252.5 2.0 collective-permute-start.7
  254.4 4.1 %collective-permute-start.8 = (bf16[2,512,128]{2,1,0:T(8,128)(2,1)S(1)}, bf16[2,512,128]{2,1,0:T(8,128)(2,1)S(1)}, u32[]{:S(2)}, u32[]{:S(2)}) collective-permute-start(bf16[2,512,128]{2,1,0:T(8,128)(2,1)S(1)} %bitcast.29), channel_id=1, source_target_pairs={{0,448},{32,480},{64,128},{96,160},{128,64},{160,96},{192,256},{22... | collective-permute-start | bytes 786440 | tf_op jit(solution)/shard_map/ppermute | solution.py:209
  258.6 12.5 %collective-permute-done.7.refs_3_ = bf16[2,512,128]{2,1,0:T(8,128)(2,1)S(1)} collective-permute-done((bf16[2,512,128]{2,1,0:T(8,128)(2,1)S(1)}, bf16[2,512,128]{2,1,0:T(8,128)(2,1)S(1)}, u32[]{:S(2)}, u32[]{:S(2)}) %collective-permute-start.7) | collective-permute-done | bytes 262176 | tf_op jit(solution)/shard_map/ppermute | solution.py:209
  271.1 2.4 down.3
  273.5 4.8 %all-to-all-start.2 = ((bf16[32,16,128]{2,1,0:T(8,128)(2,1)}), bf16[32,16,128]{2,1,0:T(8,128)(2,1)S(1)}, u32[]{:S(2)}, u32[]{:S(2)}) async-start(bf16[32,16,128]{2,1,0:T(8,128)(2,1)} %bitcast.17), calls=%async_computation.2 | async-start | bytes 262144 | tf_op jit(solution)/shard_map/all_to_all | solution.py:191
  278.3 1.6 comb.1
  279.9 14.8 %all-to-all-done.2 = bf16[32,16,128]{2,1,0:T(8,128)(2,1)S(1)} async-done(((bf16[32,16,128]{2,1,0:T(8,128)(2,1)}), bf16[32,16,128]{2,1,0:T(8,128)(2,1)S(1)}, u32[]{:S(2)}, u32[]{:S(2)}) %all-to-all-start.2) | async-done | bytes 131104 | tf_op jit(solution)/shard_map/all_to_all | solution.py:191
  294.6 0.9 copy-done
  295.5 0.9 copy-done.1
  296.4 0.9 combine.1
  (12 shorter events, 0.1 us)
Async XLA Ops:
  0.7 0.7 copy-start.2
  37.9 0.7 copy-start.3
  92.0 127.2 %collective-permute-start.4 = (bf16[32,96,128]{2,1,0:T(8,128)(2,1)S(1)}, bf16[32,96,128]{2,1,0:T(8,128)(2,1)S(1)}, u32[]{:S(2)}, u32[]{:S(2)}) collective-permute-start(bf16[32,96,128]{2,1,0:T(8,128)(2,1)S(1)} %all_to_all.15.refs_5_), channel_id=1, source_target_pairs={{0,512},{512,0},{1,513},{513,1},{2,514},{514,2},{3,515},{515,3},{4... | collective-permute-start | bytes 2359304 | tf_op jit(solution)/shard_map/ppermute | solution.py:230
  191.4 27.8 %collective-permute-start = (bf16[4,512,128]{2,1,0:T(8,128)(2,1)S(1)}, bf16[4,512,128]{2,1,0:T(8,128)(2,1)S(1)}, u32[]{:S(2)}, u32[]{:S(2)}) collective-permute-start(bf16[4,512,128]{2,1,0:T(8,128)(2,1)S(1)} %bitcast.24), channel_id=1, source_target_pairs={{0,32},{32,0},{64,96},{96,64},{128,160},{160,128},{192,224},{224,1... | collective-permute-start | bytes 1572872 | tf_op jit(solution)/shard_map/ppermute | solution.py:209
  193.4 25.8 %collective-permute-start.1 = (bf16[4,512,128]{2,1,0:T(8,128)(2,1)S(1)}, bf16[4,512,128]{2,1,0:T(8,128)(2,1)S(1)}, u32[]{:S(2)}, u32[]{:S(2)}) collective-permute-start(bf16[4,512,128]{2,1,0:T(8,128)(2,1)S(1)} %bitcast.25), channel_id=1, source_target_pairs={{0,480},{32,64},{64,32},{96,128},{128,96},{160,192},{192,160},{224... | collective-permute-start | bytes 1572872 | tf_op jit(solution)/shard_map/ppermute | solution.py:209
  195.3 23.9 %collective-permute-start.2 = (bf16[2,512,128]{2,1,0:T(8,128)(2,1)S(1)}, bf16[2,512,128]{2,1,0:T(8,128)(2,1)S(1)}, u32[]{:S(2)}, u32[]{:S(2)}) collective-permute-start(bf16[2,512,128]{2,1,0:T(8,128)(2,1)S(1)} %bitcast.28), channel_id=1, source_target_pairs={{0,64},{32,96},{64,0},{96,32},{128,192},{160,224},{192,128},{224,1... | collective-permute-start | bytes 786440 | tf_op jit(solution)/shard_map/ppermute | solution.py:209
  200.7 18.5 %collective-permute-start.3 = (bf16[2,512,128]{2,1,0:T(8,128)(2,1)S(1)}, bf16[2,512,128]{2,1,0:T(8,128)(2,1)S(1)}, u32[]{:S(2)}, u32[]{:S(2)}) collective-permute-start(bf16[2,512,128]{2,1,0:T(8,128)(2,1)S(1)} %bitcast.27), channel_id=1, source_target_pairs={{0,448},{32,480},{64,128},{96,160},{128,64},{160,96},{192,256},{22... | collective-permute-start | bytes 786440 | tf_op jit(solution)/shard_map/ppermute | solution.py:209
  244.7 26.4 %collective-permute-start.5 = (bf16[4,512,128]{2,1,0:T(8,128)(2,1)S(1)}, bf16[4,512,128]{2,1,0:T(8,128)(2,1)S(1)}, u32[]{:S(2)}, u32[]{:S(2)}) collective-permute-start(bf16[4,512,128]{2,1,0:T(8,128)(2,1)S(1)} %bitcast.19), channel_id=1, source_target_pairs={{0,32},{32,0},{64,96},{96,64},{128,160},{160,128},{192,224},{224,1... | collective-permute-start | bytes 1572872 | tf_op jit(solution)/shard_map/ppermute | solution.py:209
  248.4 22.7 %collective-permute-start.6 = (bf16[4,512,128]{2,1,0:T(8,128)(2,1)S(1)}, bf16[4,512,128]{2,1,0:T(8,128)(2,1)S(1)}, u32[]{:S(2)}, u32[]{:S(2)}) collective-permute-start(bf16[4,512,128]{2,1,0:T(8,128)(2,1)S(1)} %bitcast.20), channel_id=1, source_target_pairs={{0,480},{32,64},{64,32},{96,128},{128,96},{160,192},{192,160},{224... | collective-permute-start | bytes 1572872 | tf_op jit(solution)/shard_map/ppermute | solution.py:209
  252.5 18.6 %collective-permute-start.7 = (bf16[2,512,128]{2,1,0:T(8,128)(2,1)S(1)}, bf16[2,512,128]{2,1,0:T(8,128)(2,1)S(1)}, u32[]{:S(2)}, u32[]{:S(2)}) collective-permute-start(bf16[2,512,128]{2,1,0:T(8,128)(2,1)S(1)} %bitcast.30), channel_id=1, source_target_pairs={{0,64},{32,96},{64,0},{96,32},{128,192},{160,224},{192,128},{224,1... | collective-permute-start | bytes 786440 | tf_op jit(solution)/shard_map/ppermute | solution.py:209
  254.4 16.6 %collective-permute-start.8 = (bf16[2,512,128]{2,1,0:T(8,128)(2,1)S(1)}, bf16[2,512,128]{2,1,0:T(8,128)(2,1)S(1)}, u32[]{:S(2)}, u32[]{:S(2)}) collective-permute-start(bf16[2,512,128]{2,1,0:T(8,128)(2,1)S(1)} %bitcast.29), channel_id=1, source_target_pairs={{0,448},{32,480},{64,128},{96,160},{128,64},{160,96},{192,256},{22... | collective-permute-start | bytes 786440 | tf_op jit(solution)/shard_map/ppermute | solution.py:209
  273.5 21.1 %all-to-all-start.2 = ((bf16[32,16,128]{2,1,0:T(8,128)(2,1)}), bf16[32,16,128]{2,1,0:T(8,128)(2,1)S(1)}, u32[]{:S(2)}, u32[]{:S(2)}) async-start(bf16[32,16,128]{2,1,0:T(8,128)(2,1)} %bitcast.17), calls=%async_computation.2 | async-start | bytes 262144 | tf_op jit(solution)/shard_map/all_to_all | solution.py:191
  294.6 0.9 copy-start
  295.5 0.9 copy-start.1

commit v6 on v5

--- a/solution.py
+++ b/solution.py
@@ -99,10 +99,12 @@
     return out
 
 
-def pack_kernel(group, gate, up, down, gain, out):
-    size = gain.shape[0]
-    out[:, :size, :] = (gate[...] * gain[...]).astype(BF16)
-    out[:, size : 2 * size, :] = (up[...] * gain[...]).astype(BF16)
+def pack_kernel(group, gate, up, down, gain, out, column):
+    size, width = gate.shape[1:]
+    column[...] = jnp.broadcast_to(gain[...], (width, gain.shape[1])).T
+    scale = column[pl.ds(pl.multiple_of(group[0] * size, size), size), :]
+    out[:, :size, :] = (gate[...] * scale).astype(BF16)
+    out[:, size : 2 * size, :] = (up[...] * scale).astype(BF16)
     out[:, 2 * size :, :] = down[...].astype(BF16)
 
 
@@ -114,7 +116,7 @@
     five, weights = refs[:5], refs[5 : 5 + parts]
     hidden, gate_out, up_out, whole, sems = refs[5 + parts :]
     rows, width = hidden.shape
-    size = weights[0].shape[1] // 3
+    size = weights[0].shape[1] // 2
     copies = []
     for k, w in enumerate(weights):
         at = part_at(ids[1], k, parts, size)
@@ -158,13 +160,12 @@
     five, weights = refs[:5], refs[5 : 5 + parts]
     out, down_out, whole, sems = refs[5 + parts :]
     rows, _ = out.shape
-    size = weights[0].shape[1] // 3
+    size = weights[0].shape[1]
     copies = []
     for k, w in enumerate(weights):
         at = part_at(ids[1], k, parts, size)
-        src = w.at[:, 2 * size :, :]
-        copies.append(pltpu.make_async_copy(src, down_out.at[:, at, :], sems.at[k]))
-        whole[:, at, :] = w[:, 2 * size :, :]
+        copies.append(pltpu.make_async_copy(w, down_out.at[:, at, :], sems.at[k]))
+        whole[:, at, :] = w[...]
     for c in copies:
         c.start()
     order = pieces(*five, ids[0], stride)
@@ -283,22 +284,25 @@
 
     size = gate_train.shape[1] // parts
 
-    step = 8
+    step = 16
     taken = (step, size, gate_train.shape[2])
     train_spec = pl.BlockSpec(taken, lambda i, group: (i, group[0], 0))
-    gain = jnp.broadcast_to(norm_gain[:, None], (norm_gain.shape[0], taken[2]))
+    rows = norm_gain.shape[0]
     packed = pl.pallas_call(
         pack_kernel,
         grid_spec=pltpu.PrefetchScalarGridSpec(
             num_scalar_prefetch=1,
             grid=(EXPERTS // step,),
-            in_specs=[train_spec] * 3 + [pl.BlockSpec(taken[1:], lambda i, group: (group[0], 0))],
+            in_specs=[train_spec] * 3 + [pl.BlockSpec((1, rows), lambda i, group: (0, 0))],
             out_specs=pl.BlockSpec((step, 3 * size, taken[2]), lambda i, group: (i, 0, 0)),
+            scratch_shapes=[pltpu.VMEM((rows, taken[2]), F32)],
         ),
         out_shape=jax.ShapeDtypeStruct((EXPERTS, 3 * size, taken[2]), BF16),
         name="pack",
-    )(my_group.reshape(1), gate_train, up_train, down_train, gain)
-    weights = in_vmem(other_groups(exchange(after(packed, arrived))))
+    )(my_group.reshape(1), gate_train, up_train, down_train, norm_gain.reshape(1, rows))
+    served_part = exchange(after(packed, arrived))
+    both = in_vmem(other_groups(served_part[:, : 2 * size]))
+    downs = in_vmem(other_groups(served_part[:, 2 * size :]))
     served = jax.ShapeDtypeStruct(down_train.shape, BF16)
     hbm = pl.BlockSpec(memory_space=pl.ANY)
 
@@ -325,7 +329,7 @@
         ],
         compiler_params=pltpu.CompilerParams(vmem_limit_bytes=16 << 20),
         name="gate_up",
-    )(ids, *in_vmem(token_blocks), *weights)
+    )(ids, *in_vmem(token_blocks), *both)
     expert_out, down_serve = pl.pallas_call(
         functools.partial(down_kernel, stride=stride, parts=parts),
         in_specs=[sm()] + [vm()] * (5 + parts),
@@ -337,7 +341,7 @@
         ],
         compiler_params=pltpu.CompilerParams(vmem_limit_bytes=16 << 20),
         name="down",
-    )(ids, *in_vmem(gather(hidden)), *weights)
+    )(ids, *in_vmem(gather(hidden)), *downs)
     returned = exchange(expert_out.reshape(tp_count, slots // tp_count, -1)).reshape(slots, -1)
     mixed = pl.pallas_call(
         combine_kernel,

time: 300 us -> 263 us (0.88)
  starting transfers between devices: 104 us -> 69.9 us
  waiting for transfers between devices: 43.7 us -> 37.4 us
  blocking collectives: 132 us -> 138 us
    all_gather x2, blocking collectives: 48.8 us -> 104 us  [strided(): return lax.all_gather(x, 'fs', axis=0, axis_index_groups=groups)]
    all_to_all x2 -> x1, blocking collectives: 83.7 us -> 34.5 us  [exchange(): return lax.all_to_all(x, 'tp', split_axis=0, concat_axis=0, tiled=True)]
    ppermute x1 -> x2, starting transfers between devices: 73.9 us -> 26.8 us  [other_groups(): lax.ppermute(x, 'grp', [(i, (i + k) % count) for i in range(count)])]
    ppermute x8, starting transfers between devices: 25.1 us -> 31.7 us  [swap(): lax.ppermute(x, 'fs', [(i, partner(i) % count) for i in range(count)])]
    all_to_all x1 -> x2, starting transfers between devices: 4.77 us -> 11.4 us  [exchange(): return lax.all_to_all(x, 'tp', split_axis=0, concat_axis=0, tiled=True)]
    ppermute x8, waiting for transfers between devices: 28.9 us -> 22.5 us  [swap(): lax.ppermute(x, 'fs', [(i, partner(i) % count) for i in range(count)])]
    all_to_all x1 -> x2, waiting for transfers between devices: 14.8 us -> 14.9 us  [exchange(): return lax.all_to_all(x, 'tp', split_axis=0, concat_axis=0, tiled=True)]
  transfers between devices with their start and end apart: 10 -> 12, of which waited for: 3 -> 5; matrix products, arithmetic and copies ran while one was open for 0% -> 0% of each run, Pallas kernels for 1% -> 1%
where the time goes in v6:
time: 263 us; the launch traced here: 260 us
  blocking collectives  138 us (52%)
  starting transfers between devices  69.9 us (27%)
  waiting for transfers between devices  37.4 us (14%)
  Pallas kernels  11.5 us (4%)
    all_gather x2, blocking collectives, strided(): return lax.all_gather(x, 'fs', axis=0, axis_index_groups=groups)  104 us
    all_to_all x1, blocking collectives, exchange(): return lax.all_to_all(x, 'tp', split_axis=0, concat_axis=0, tiled=True)  34.5 us
    ppermute x8, starting transfers between devices, swap(): lax.ppermute(x, 'fs', [(i, partner(i) % count) for i in range(count)])  31.7 us
    ppermute x2, starting transfers between devices, other_groups(): lax.ppermute(x, 'grp', [(i, (i + k) % count) for i in range(count)])  26.8 us
    ppermute x8, waiting for transfers between devices, swap(): lax.ppermute(x, 'fs', [(i, partner(i) % count) for i in range(count)])  22.5 us
    all_to_all x2, waiting for transfers between devices, exchange(): return lax.all_to_all(x, 'tp', split_axis=0, concat_axis=0, tiled=True)  14.9 us
    all_to_all x2, starting transfers between devices, exchange(): return lax.all_to_all(x, 'tp', split_axis=0, concat_axis=0, tiled=True)  11.4 us
  transfers between devices with their start and end apart: 12, of which 5 were waited for; matrix products, arithmetic and copies ran while one was open for 0% of the time, Pallas kernels for 1%

profile of v6, /device:TPU:6, one launch (start us, length us, event | category | flops | bytes accessed | tf_op | source)
XLA Modules:
  0.0 260.4 jit_solution(8375339941677162022)
XLA Ops:
  0.7 0.6 copy-done.2
  1.3 36.6 %conditional.1 = (bf16[32,24,128]{2,1,0:T(8,128)(2,1)S(1)}) conditional(s32[]{:T(128)} %convert_element_type.3, () %tuple.15, (s32[3]{0:T(128)S(1)}, bf16[120,2048]{1,0:T(8,128)(2,1)}, s32[4,120]{1,0:T(4,128)S(1)}) %tuple.22), branch_computations={%region_0.1_spmd, %region_1.2_spmd} | conditional | bytes 393224 | solution.py:276
  1.3 2.1 prep.1
  3.5 34.5 %all_to_all.14 = bf16[32,24,128]{2,1,0:T(8,128)(2,1)S(1)} all-to-all(bf16[32,24,128]{2,1,0:T(8,128)(2,1)} %prep.1), channel_id=1, replica_groups=mesh['grp'=2,'fs'=16,'tp'=32] {'tp'}, dimensions={0} | all-to-all | bytes 393216 | tf_op jit(solution)/shard_map/cond/branch_1_fun/all_to_all | solution.py:192
  37.9 2.2 pack.1
  40.2 4.8 %all-to-all-start.1 = ((bf16[32,96,128]{2,1,0:T(8,128)(2,1)}), bf16[32,96,128]{2,1,0:T(8,128)(2,1)S(1)}, u32[]{:S(2)}, u32[]{:S(2)}) async-start(bf16[32,96,128]{2,1,0:T(8,128)(2,1)} %pack.1), calls=%async_computation.1 | async-start | bytes 1572864 | tf_op jit(solution)/shard_map/all_to_all | solution.py:192
  45.0 79.4 %all-gather = bf16[128,24,128]{2,1,0:T(8,128)(2,1)S(1)} all-gather(bf16[32,24,128]{2,1,0:T(8,128)(2,1)S(1)} %get-tuple-element.42), channel_id=2, replica_groups={{0,128,256,384},{32,160,288,416},{64,192,320,448},{96,224,352,480},{1,1..., dimensions={0}, use_global_device_ids=true | all-gather | bytes 983040 | tf_op jit(solution)/shard_map/all_gather | solution.py:203
  124.4 0.1 repack.1
  124.6 12.3 %collective-permute-start.1 = (bf16[4,512,128]{2,1,0:T(8,128)(2,1)S(1)}, bf16[4,512,128]{2,1,0:T(8,128)(2,1)S(1)}, u32[]{:S(2)}, u32[]{:S(2)}) collective-permute-start(bf16[4,512,128]{2,1,0:T(8,128)(2,1)S(1)} %bitcast.25), channel_id=1, source_target_pairs={{0,480},{32,64},{64,32},{96,128},{128,96},{160,192},{192,160},{224... | collective-permute-start | bytes 1572872 | tf_op jit(solution)/shard_map/ppermute | solution.py:210
  136.9 2.5 collective-permute-start
  139.5 23.9 %collective-permute-start.4 = (bf16[32,64,128]{2,1,0:T(8,128)(2,1)S(1)}, bf16[32,64,128]{2,1,0:T(8,128)(2,1)S(1)}, u32[]{:S(2)}, u32[]{:S(2)}) collective-permute-start(bf16[32,64,128]{2,1,0:T(8,128)(2,1)S(1)} %slice.18.refs_5_), channel_id=1, source_target_pairs={{0,512},{512,0},{1,513},{513,1},{2,514},{514,2},{3,515},{515,3},{4... | collective-permute-start | bytes 1572872 | tf_op jit(solution)/shard_map/ppermute | solution.py:231
  163.4 2.0 collective-permute-start.2
  165.3 2.0 collective-permute-start.3
  167.3 0.1 pad_add_fusion.ids
  167.4 6.4 %collective-permute-done.2.refs_3_ = bf16[2,512,128]{2,1,0:T(8,128)(2,1)S(1)} collective-permute-done((bf16[2,512,128]{2,1,0:T(8,128)(2,1)S(1)}, bf16[2,512,128]{2,1,0:T(8,128)(2,1)S(1)}, u32[]{:S(2)}, u32[]{:S(2)}) %collective-permute-start.2) | collective-permute-done | bytes 262176 | tf_op jit(solution)/shard_map/ppermute | solution.py:210
  173.7 3.2 %collective-permute-done.3.refs_4_ = bf16[2,512,128]{2,1,0:T(8,128)(2,1)S(1)} collective-permute-done((bf16[2,512,128]{2,1,0:T(8,128)(2,1)S(1)}, bf16[2,512,128]{2,1,0:T(8,128)(2,1)S(1)}, u32[]{:S(2)}, u32[]{:S(2)}) %collective-permute-start.3) | collective-permute-done | bytes 262176 | tf_op jit(solution)/shard_map/ppermute | solution.py:210
  176.9 2.1 gate_up.1
  179.0 24.2 %all-gather.1 = bf16[2048,128]{1,0:T(8,128)(2,1)S(1)} all-gather(bf16[512,128]{1,0:T(8,128)(2,1)S(1)} %get-tuple-element.33), channel_id=3, replica_groups={{0,128,256,384},{32,160,288,416},{64,192,320,448},{96,224,352,480},{1,1..., dimensions={0}, use_global_device_ids=true | all-gather | bytes 655360 | tf_op jit(solution)/shard_map/all_gather | solution.py:203
  203.2 1.9 collective-permute-start.6
  205.1 4.5 %collective-permute-start.5 = (bf16[4,512,128]{2,1,0:T(8,128)(2,1)S(1)}, bf16[4,512,128]{2,1,0:T(8,128)(2,1)S(1)}, u32[]{:S(2)}, u32[]{:S(2)}) collective-permute-start(bf16[4,512,128]{2,1,0:T(8,128)(2,1)S(1)} %bitcast.21), channel_id=1, source_target_pairs={{0,32},{32,0},{64,96},{96,64},{128,160},{160,128},{192,224},{224,1... | collective-permute-start | bytes 1572872 | tf_op jit(solution)/shard_map/ppermute | solution.py:210
  209.7 2.9 %collective-permute-start.9 = (bf16[32,32,128]{2,1,0:T(8,128)(2,1)S(1)}, bf16[32,32,128]{2,1,0:T(8,128)(2,1)S(1)}, u32[]{:S(2)}, u32[]{:S(2)}) collective-permute-start(bf16[32,32,128]{2,1,0:T(8,128)(2,1)S(1)} %slice.21.refs_5_), channel_id=1, source_target_pairs={{0,512},{512,0},{1,513},{513,1},{2,514},{514,2},{3,515},{515,3},{4... | collective-permute-start | bytes 786440 | tf_op jit(solution)/shard_map/ppermute | solution.py:231
  212.6 3.3 %collective-permute-start.7 = (bf16[2,512,128]{2,1,0:T(8,128)(2,1)S(1)}, bf16[2,512,128]{2,1,0:T(8,128)(2,1)S(1)}, u32[]{:S(2)}, u32[]{:S(2)}) collective-permute-start(bf16[2,512,128]{2,1,0:T(8,128)(2,1)S(1)} %bitcast.31), channel_id=1, source_target_pairs={{0,64},{32,96},{64,0},{96,32},{128,192},{160,224},{192,128},{224,1... | collective-permute-start | bytes 786440 | tf_op jit(solution)/shard_map/ppermute | solution.py:210
  215.9 3.3 %collective-permute-start.8 = (bf16[2,512,128]{2,1,0:T(8,128)(2,1)S(1)}, bf16[2,512,128]{2,1,0:T(8,128)(2,1)S(1)}, u32[]{:S(2)}, u32[]{:S(2)}) collective-permute-start(bf16[2,512,128]{2,1,0:T(8,128)(2,1)S(1)} %bitcast.30), channel_id=1, source_target_pairs={{0,448},{32,480},{64,128},{96,160},{128,64},{160,96},{192,256},{22... | collective-permute-start | bytes 786440 | tf_op jit(solution)/shard_map/ppermute | solution.py:210
  219.2 11.0 %collective-permute-done.7.refs_3_ = bf16[2,512,128]{2,1,0:T(8,128)(2,1)S(1)} collective-permute-done((bf16[2,512,128]{2,1,0:T(8,128)(2,1)S(1)}, bf16[2,512,128]{2,1,0:T(8,128)(2,1)S(1)}, u32[]{:S(2)}, u32[]{:S(2)}) %collective-permute-start.7) | collective-permute-done | bytes 262176 | tf_op jit(solution)/shard_map/ppermute | solution.py:210
  230.2 1.9 collective-permute-done.8.refs_4_
  232.2 2.4 down.3
  234.6 6.6 %all-to-all-start.2 = ((bf16[32,16,128]{2,1,0:T(8,128)(2,1)}), bf16[32,16,128]{2,1,0:T(8,128)(2,1)S(1)}, u32[]{:S(2)}, u32[]{:S(2)}) async-start(bf16[32,16,128]{2,1,0:T(8,128)(2,1)} %bitcast.18), calls=%async_computation.2 | async-start | bytes 262144 | tf_op jit(solution)/shard_map/all_to_all | solution.py:192
  241.2 1.6 comb.1
  242.8 14.9 %all-to-all-done.2 = bf16[32,16,128]{2,1,0:T(8,128)(2,1)S(1)} async-done(((bf16[32,16,128]{2,1,0:T(8,128)(2,1)}), bf16[32,16,128]{2,1,0:T(8,128)(2,1)S(1)}, u32[]{:S(2)}, u32[]{:S(2)}) %all-to-all-start.2) | async-done | bytes 131104 | tf_op jit(solution)/shard_map/all_to_all | solution.py:192
  257.7 0.9 copy-done
  258.6 0.9 copy-done.1
  259.5 0.9 combine.1
  (14 shorter events, 0.2 us)
Async XLA Ops:
  0.7 0.7 copy-start.2
  40.2 99.2 %all-to-all-start.1 = ((bf16[32,96,128]{2,1,0:T(8,128)(2,1)}), bf16[32,96,128]{2,1,0:T(8,128)(2,1)S(1)}, u32[]{:S(2)}, u32[]{:S(2)}) async-start(bf16[32,96,128]{2,1,0:T(8,128)(2,1)} %pack.1), calls=%async_computation.1 | async-start | bytes 1572864 | tf_op jit(solution)/shard_map/all_to_all | solution.py:192
  124.6 52.3 %collective-permute-start.1 = (bf16[4,512,128]{2,1,0:T(8,128)(2,1)S(1)}, bf16[4,512,128]{2,1,0:T(8,128)(2,1)S(1)}, u32[]{:S(2)}, u32[]{:S(2)}) collective-permute-start(bf16[4,512,128]{2,1,0:T(8,128)(2,1)S(1)} %bitcast.25), channel_id=1, source_target_pairs={{0,480},{32,64},{64,32},{96,128},{128,96},{160,192},{192,160},{224... | collective-permute-start | bytes 1572872 | tf_op jit(solution)/shard_map/ppermute | solution.py:210
  136.9 40.0 %collective-permute-start = (bf16[4,512,128]{2,1,0:T(8,128)(2,1)S(1)}, bf16[4,512,128]{2,1,0:T(8,128)(2,1)S(1)}, u32[]{:S(2)}, u32[]{:S(2)}) collective-permute-start(bf16[4,512,128]{2,1,0:T(8,128)(2,1)S(1)} %bitcast.26), channel_id=1, source_target_pairs={{0,32},{32,0},{64,96},{96,64},{128,160},{160,128},{192,224},{224,1... | collective-permute-start | bytes 1572872 | tf_op jit(solution)/shard_map/ppermute | solution.py:210
  139.5 37.4 %collective-permute-start.4 = (bf16[32,64,128]{2,1,0:T(8,128)(2,1)S(1)}, bf16[32,64,128]{2,1,0:T(8,128)(2,1)S(1)}, u32[]{:S(2)}, u32[]{:S(2)}) collective-permute-start(bf16[32,64,128]{2,1,0:T(8,128)(2,1)S(1)} %slice.18.refs_5_), channel_id=1, source_target_pairs={{0,512},{512,0},{1,513},{513,1},{2,514},{514,2},{3,515},{515,3},{4... | collective-permute-start | bytes 1572872 | tf_op jit(solution)/shard_map/ppermute | solution.py:231
  163.4 10.4 %collective-permute-start.2 = (bf16[2,512,128]{2,1,0:T(8,128)(2,1)S(1)}, bf16[2,512,128]{2,1,0:T(8,128)(2,1)S(1)}, u32[]{:S(2)}, u32[]{:S(2)}) collective-permute-start(bf16[2,512,128]{2,1,0:T(8,128)(2,1)S(1)} %bitcast.29), channel_id=1, source_target_pairs={{0,64},{32,96},{64,0},{96,32},{128,192},{160,224},{192,128},{224,1... | collective-permute-start | bytes 786440 | tf_op jit(solution)/shard_map/ppermute | solution.py:210
  165.3 11.6 %collective-permute-start.3 = (bf16[2,512,128]{2,1,0:T(8,128)(2,1)S(1)}, bf16[2,512,128]{2,1,0:T(8,128)(2,1)S(1)}, u32[]{:S(2)}, u32[]{:S(2)}) collective-permute-start(bf16[2,512,128]{2,1,0:T(8,128)(2,1)S(1)} %bitcast.28), channel_id=1, source_target_pairs={{0,448},{32,480},{64,128},{96,160},{128,64},{160,96},{192,256},{22... | collective-permute-start | bytes 786440 | tf_op jit(solution)/shard_map/ppermute | solution.py:210
  203.2 29.0 %collective-permute-start.6 = (bf16[4,512,128]{2,1,0:T(8,128)(2,1)S(1)}, bf16[4,512,128]{2,1,0:T(8,128)(2,1)S(1)}, u32[]{:S(2)}, u32[]{:S(2)}) collective-permute-start(bf16[4,512,128]{2,1,0:T(8,128)(2,1)S(1)} %bitcast.20), channel_id=1, source_target_pairs={{0,480},{32,64},{64,32},{96,128},{128,96},{160,192},{192,160},{224... | collective-permute-start | bytes 1572872 | tf_op jit(solution)/shard_map/ppermute | solution.py:210
  205.1 27.0 %collective-permute-start.5 = (bf16[4,512,128]{2,1,0:T(8,128)(2,1)S(1)}, bf16[4,512,128]{2,1,0:T(8,128)(2,1)S(1)}, u32[]{:S(2)}, u32[]{:S(2)}) collective-permute-start(bf16[4,512,128]{2,1,0:T(8,128)(2,1)S(1)} %bitcast.21), channel_id=1, source_target_pairs={{0,32},{32,0},{64,96},{96,64},{128,160},{160,128},{192,224},{224,1... | collective-permute-start | bytes 1572872 | tf_op jit(solution)/shard_map/ppermute | solution.py:210
  209.7 9.5 %collective-permute-start.9 = (bf16[32,32,128]{2,1,0:T(8,128)(2,1)S(1)}, bf16[32,32,128]{2,1,0:T(8,128)(2,1)S(1)}, u32[]{:S(2)}, u32[]{:S(2)}) collective-permute-start(bf16[32,32,128]{2,1,0:T(8,128)(2,1)S(1)} %slice.21.refs_5_), channel_id=1, source_target_pairs={{0,512},{512,0},{1,513},{513,1},{2,514},{514,2},{3,515},{515,3},{4... | collective-permute-start | bytes 786440 | tf_op jit(solution)/shard_map/ppermute | solution.py:231
  212.6 17.6 %collective-permute-start.7 = (bf16[2,512,128]{2,1,0:T(8,128)(2,1)S(1)}, bf16[2,512,128]{2,1,0:T(8,128)(2,1)S(1)}, u32[]{:S(2)}, u32[]{:S(2)}) collective-permute-start(bf16[2,512,128]{2,1,0:T(8,128)(2,1)S(1)} %bitcast.31), channel_id=1, source_target_pairs={{0,64},{32,96},{64,0},{96,32},{128,192},{160,224},{192,128},{224,1... | collective-permute-start | bytes 786440 | tf_op jit(solution)/shard_map/ppermute | solution.py:210
  215.9 16.2 %collective-permute-start.8 = (bf16[2,512,128]{2,1,0:T(8,128)(2,1)S(1)}, bf16[2,512,128]{2,1,0:T(8,128)(2,1)S(1)}, u32[]{:S(2)}, u32[]{:S(2)}) collective-permute-start(bf16[2,512,128]{2,1,0:T(8,128)(2,1)S(1)} %bitcast.30), channel_id=1, source_target_pairs={{0,448},{32,480},{64,128},{96,160},{128,64},{160,96},{192,256},{22... | collective-permute-start | bytes 786440 | tf_op jit(solution)/shard_map/ppermute | solution.py:210
  234.6 23.1 %all-to-all-start.2 = ((bf16[32,16,128]{2,1,0:T(8,128)(2,1)}), bf16[32,16,128]{2,1,0:T(8,128)(2,1)S(1)}, u32[]{:S(2)}, u32[]{:S(2)}) async-start(bf16[32,16,128]{2,1,0:T(8,128)(2,1)} %bitcast.18), calls=%async_computation.2 | async-start | bytes 262144 | tf_op jit(solution)/shard_map/all_to_all | solution.py:192
  257.7 0.9 copy-start
  258.6 0.9 copy-start.1
